TPU v7x, 512 devices: a 4x2x32 block of a 4x8x32 slice. The times are simulated.
512 devices in a mesh: grp: 2 (over y), ra: 32 (over z), cb: 8 (over x, core).
Axes of the slice: x: 4, y: 2, z: 32, core: 2. Of those that a mesh axis runs over, the one named last changes fastest.
The devices are a block of a 4x8x32 slice.
Arguments:
- tokens: bfloat16 [512, 4096], P('grp', 'cb'), parts along dimension 0, may hold values from -50 to 50
- norm_gains: float32 [3, 4096], P(None, 'cb'), may hold values from 0.1 to 1.9
- gate_weight: float32 [2, 4096, 11264], P(None, 'cb', 'ra'), may hold values from -0.09375 to 0.09375
- value_weight: float32 [2, 4096, 11264], P(None, 'cb', 'ra'), may hold values from -0.09375 to 0.09375
- gate_scale: float32 [2, 11264], P(None, 'ra'), may hold values from 0.3 to 3
- value_scale: float32 [2, 11264], P(None, 'ra'), may hold values from 0.3 to 3
- conv_gate: float32 [2, 3, 11264], P(None, None, 'ra'), may hold values from -3 to 3
- conv_value: float32 [2, 3, 11264], P(None, None, 'ra'), may hold values from -3 to 3
- down_weight: float32 [2, 11264, 4096], P(None, 'ra', 'cb'), may hold values from -0.07537784 to 0.07537784
- down_scale: float32 [2, 4096], P(None, 'cb'), may hold values from 0.3 to 3
Outputs:
- normed_out: bfloat16 [512, 4096], P('grp', 'cb'), parts along dimension 0
There are 2 independent parts, one for each index of `grp`. A program takes and returns all parts, laid end to end along the dimension named above; an argument that names none is the same for every part. Nothing has to cross between parts.
All inputs are finite; a program needn't handle non-finite values.
Results may differ from a plain program's by a relative error of at most 0.012.
The roundings to bfloat16 on the way count: a program that leaves them out, or rounds other values in their place, can miss the bound.
Values may be sent and summed in bfloat16 or wider, within the bound.
A program may use at most 64 MiB of HBM per device.

v0:
```python
import jax
import jax.numpy as jnp
from jax import lax
from jax.sharding import PartitionSpec as P

epsilon = 1e-06
residual_weight = 0.5


def copy_for_each(array, axis):
    copies = jnp.broadcast_to(array, (lax.axis_size(axis), *array.shape))
    return lax.all_to_all(copies, axis, split_axis=0, concat_axis=0, tiled=True)


def taken_together(array, axis):
    return copy_for_each(array, axis).sum(axis=0)


def packed_total(arrays, axis):
    ravelled, at, outs = (jnp.concatenate([a.reshape(-1) for a in arrays]), 0, [])
    total = taken_together(ravelled, axis)
    for a in arrays:
        outs.append(total[at : at + a.size].reshape(a.shape))
        at += a.size
    return tuple(outs)


def filled_up(lines, size):
    spare = -len(lines) % size
    return jnp.pad(lines, [(0, spare)] + [(0, 0)] * (lines.ndim - 1))


def sum_in_two_steps(array, axis):
    lines = array.reshape(-1, *array.shape[1:][-1:])
    padded = filled_up(lines, lax.axis_size(axis))
    own = lax.psum_scatter(padded, axis, scatter_dimension=0, tiled=True)
    whole = lax.all_gather(own, axis, axis=0, tiled=True)
    return whole[: len(lines)].reshape(array.shape)


def causal_taps(projected, tap_weights):
    tap_count = tap_weights.shape[0]
    row_count = projected.shape[0]
    padded = jnp.pad(projected, ((tap_count - 1, 0), (0, 0)))
    result = jnp.zeros_like(projected)
    for tap_idx in range(tap_count):
        result = result + padded[tap_idx : tap_idx + row_count] * tap_weights[tap_idx]
    return result


def row_inverse(state_wide, model_width):
    squares = taken_together(jnp.sum(state_wide * state_wide, axis=1, keepdims=True), "cb")
    return lax.rsqrt(squares / model_width + epsilon)


def on_device(
    tokens,
    norm_gains,
    gate_weight,
    value_weight,
    gate_scale,
    value_scale,
    conv_gate,
    conv_value,
    down_weight,
    down_scale,
):
    model_width = lax.axis_size("cb") * tokens.shape[1]
    layer_count = gate_weight.shape[0]
    current = tokens
    for layer_idx in range(layer_count):
        state_wide = current.astype(jnp.float32)
        inverse = row_inverse(state_wide, model_width)
        scaled = (state_wide * norm_gains[layer_idx]).astype(jnp.bfloat16)
        gate_part = jnp.dot(
            scaled, gate_weight[layer_idx].astype(jnp.bfloat16), preferred_element_type=jnp.float32
        )
        value_part = jnp.dot(
            scaled, value_weight[layer_idx].astype(jnp.bfloat16), preferred_element_type=jnp.float32
        )
        gate_sum, value_sum = packed_total((gate_part, value_part), "cb")
        gate_cols = gate_scale[layer_idx]
        value_cols = value_scale[layer_idx]
        gate_taps = conv_gate[layer_idx]
        value_taps = conv_value[layer_idx]
        gate_pre = inverse * gate_cols * gate_sum
        value_pre = inverse * value_cols * value_sum
        hidden = (
            jax.nn.gelu(causal_taps(gate_pre, gate_taps), approximate=True)
            * causal_taps(value_pre, value_taps)
        ).astype(jnp.bfloat16)
        partial_value = jnp.dot(
            hidden, down_weight[layer_idx].astype(jnp.bfloat16), preferred_element_type=jnp.float32
        )
        down_total = sum_in_two_steps(partial_value, "ra")
        current = (residual_weight * state_wide + down_scale[layer_idx] * down_total).astype(
            jnp.bfloat16
        )
    state_wide = current.astype(jnp.float32)
    inverse = row_inverse(state_wide, model_width)
    return (state_wide * inverse * norm_gains[layer_count]).astype(jnp.bfloat16)


def solution(mesh):
    in_specs = (
        P("grp", "cb"),
        P(None, "cb"),
        P(None, "cb", "ra"),
        P(None, "cb", "ra"),
        P(None, "ra"),
        P(None, "ra"),
        P(None, None, "ra"),
        P(None, None, "ra"),
        P(None, "ra", "cb"),
        P(None, "cb"),
    )
    out_specs = P("grp", "cb")
    return jax.shard_map(
        on_device, mesh=mesh, in_specs=in_specs, out_specs=out_specs, check_vma=False
    )
```

profile of v0, /device:TPU:40, one launch (start us, length us, event | category | flops | bytes accessed | tf_op | source)
XLA Modules:
  0.0 618.5 jit_solution(10216185116826564834)
XLA Ops:
  6.5 1.1 fusion.5
  8.3 4.6 all-to-all-start
  13.7 1.5 convert.12
  15.2 1.3 fusion.34
  16.8 1.5 convert.13
  19.0 4.0 broadcast_in_dim.19
  23.0 5.0 all-to-all-start.1
  28.1 1.0 convert.14
  29.2 65.3 %all-to-all-done.1 = f32[8,1,180224]{2,1,0:T(1,128)} async-done(((f32[8,1,180224]{2,1,0:T(1,128)}), f32[8,1,180224]{2,1,0:T(1,128)}, u32[]{:S(2)}, u32[]{:S(2)}) %all-to-all-start.1) | async-done | bytes 5767200 | tf_op jit(solution)/shard_map/all_to_all | solution.py:12
  94.5 9.7 %reduce_sum.74 = f32[180224]{0:T(1024)S(1)} reduce(f32[8,1,180224]{2,1,0:T(1,128)} %all-to-all-done.1, f32[]{:T(128)} %constant.8.clone.1), dimensions={0,1}, to_apply=%region_2.0 | reduce | flops 1261568 | bytes 6488068 | tf_op jit(solution)/shard_map/reduce_sum | solution.py:16
  104.8 2.3 fusion.32
  107.2 155.3 %reduce-scatter.3.cloned.1.call-done = f32[8,512]{1,0:T(8,128)} async-done(((f32[256,512]{1,0:T(8,128)}), f32[8,512]{1,0:T(8,128)}) %reduce-scatter.3.cloned.1.call-update) | async-done | bytes 16400 | tf_op jit(solution)/shard_map/reduce_scatter | solution.py:36
  262.6 55.8 %all_gather.6 = f32[256,512]{1,0:T(8,128)S(1)} all-gather(f32[8,512]{1,0:T(8,128)} %reduce-scatter.3.cloned.1.call-done), channel_id=1, replica_groups=mesh['grp'=2,'ra'=32,'cb'=8] {'ra'}, dimensions={0}, use_global_device_ids=true | all-gather | bytes 540672 | tf_op jit(solution)/shard_map/all_gather | solution.py:37
  320.4 4.4 all-to-all-start.2
  324.9 5.3 all-to-all-done.2
  330.1 3.9 broadcast_in_dim.21
  334.1 4.9 all-to-all-start.3
  339.1 66.3 %all-to-all-done.3 = f32[8,1,180224]{2,1,0:T(1,128)} async-done(((f32[8,1,180224]{2,1,0:T(1,128)}), f32[8,1,180224]{2,1,0:T(1,128)}, u32[]{:S(2)}, u32[]{:S(2)}) %all-to-all-start.3) | async-done | bytes 5767200 | tf_op jit(solution)/shard_map/all_to_all | solution.py:12
  405.3 9.7 %reduce_sum.77 = f32[180224]{0:T(1024)S(1)} reduce(f32[8,1,180224]{2,1,0:T(1,128)} %all-to-all-done.3, f32[]{:T(128)} %constant.8.clone.1), dimensions={0,1}, to_apply=%region_6.7 | reduce | flops 1261568 | bytes 6488068 | tf_op jit(solution)/shard_map/reduce_sum | solution.py:16
  415.6 1.3 fusion.29
  417.0 128.5 %reduce-scatter.5.cloned.1.call-done = f32[8,512]{1,0:T(8,128)} async-done(((f32[256,512]{1,0:T(8,128)}), f32[8,512]{1,0:T(8,128)}) %reduce-scatter.5.cloned.1.call-update) | async-done | bytes 16400 | tf_op jit(solution)/shard_map/reduce_scatter | solution.py:36
  545.5 55.7 %all_gather.7 = f32[256,512]{1,0:T(8,128)S(1)} all-gather(f32[8,512]{1,0:T(8,128)} %reduce-scatter.5.cloned.1.call-done), channel_id=1, replica_groups=mesh['grp'=2,'ra'=32,'cb'=8] {'ra'}, dimensions={0}, use_global_device_ids=true | all-gather | bytes 540672 | tf_op jit(solution)/shard_map/all_gather | solution.py:37
  601.4 9.4 %all_to_all.27 = f32[8,256,1]{1,2,0:T(1,128)S(1)} all-to-all(f32[8,256,1]{1,2,0:T(1,128)S(1)} %broadcast_in_dim.22), channel_id=1, replica_groups=mesh['grp'=2,'ra'=32,'cb'=8] {'cb'}, dimensions={0} | all-to-all | bytes 16384 | tf_op jit(solution)/shard_map/all_to_all | solution.py:12
  610.9 0.8 fusion.2
  (53 shorter events, 6.5 us)
Async XLA Ops:
  6.5 11.7 %copy-start = (bf16[256,512]{1,0:T(8,128)(2,1)S(1)}, bf16[256,512]{1,0:T(8,128)(2,1)}, u32[]{:S(2)}) copy-start(bf16[256,512]{1,0:T(8,128)(2,1)} %param.10) | copy-start | bytes 786436
  8.3 10.7 %all-to-all-start = ((f32[8,256,1]{1,2,0:T(1,128)}), f32[8,256,1]{1,2,0:T(1,128)S(1)}, u32[]{:S(2)}, u32[]{:S(2)}) async-start(f32[8,256,1]{1,2,0:T(1,128)} %broadcast_in_dim.18), calls=%async_computation | async-start | bytes 16384 | tf_op jit(solution)/shard_map/all_to_all | solution.py:12
  22.9 5.1 copy-start.1
  22.9 6.1 copy-start.6
  22.9 6.1 copy-start.7
  22.9 6.1 copy-start.3
  23.0 6.1 copy-start.4
  23.0 71.6 %all-to-all-start.1 = ((f32[8,1,180224]{2,1,0:T(1,128)}), f32[8,1,180224]{2,1,0:T(1,128)}, u32[]{:S(2)}, u32[]{:S(2)}) async-start(f32[8,1,180224]{2,1,0:T(1,128)} %broadcast_in_dim.19), calls=%async_computation.1 | async-start | bytes 11534336 | tf_op jit(solution)/shard_map/all_to_all | solution.py:12
  28.0 234.6 %reduce-scatter.3.cloned.1.call-start = ((), (), s32[]{:S(2)}) async-start(), calls=%async_computation.7 | async-start | bytes 540672 | tf_op jit(solution)/shard_map/reduce_scatter | solution.py:36
  29.2 78.0 %copy-start.5 = (f32[2,512]{1,0:T(2,128)S(1)}, f32[2,512]{1,0:T(2,128)}, u32[]{:S(2)}) copy-start(f32[2,512]{1,0:T(2,128)} %param.19) | copy-start | bytes 12292
  320.4 9.7 %all-to-all-start.2 = ((f32[8,256,1]{1,2,0:T(1,128)}), f32[8,256,1]{1,2,0:T(1,128)S(1)}, u32[]{:S(2)}, u32[]{:S(2)}) async-start(f32[8,256,1]{1,2,0:T(1,128)} %broadcast_in_dim.20), calls=%async_computation.3 | async-start | bytes 16384 | tf_op jit(solution)/shard_map/all_to_all | solution.py:12
  334.1 71.3 %all-to-all-start.3 = ((f32[8,1,180224]{2,1,0:T(1,128)}), f32[8,1,180224]{2,1,0:T(1,128)}, u32[]{:S(2)}, u32[]{:S(2)}) async-start(f32[8,1,180224]{2,1,0:T(1,128)} %broadcast_in_dim.21), calls=%async_computation.4 | async-start | bytes 11534336 | tf_op jit(solution)/shard_map/all_to_all | solution.py:12
  338.9 76.7 %copy-start.2 = (bf16[2,352,512]{2,1,0:T(8,128)(2,1)S(1)}, bf16[2,352,512]{2,1,0:T(8,128)(2,1)}, u32[]{:S(2)}) copy-start(bf16[2,352,512]{2,1,0:T(8,128)(2,1)} %convert.14) | copy-start | bytes 2162692
  339.0 206.6 %reduce-scatter.5.cloned.1.call-start = ((), (), s32[]{:S(2)}) async-start(), calls=%async_computation.8 | async-start | bytes 540672 | tf_op jit(solution)/shard_map/reduce_scatter | solution.py:36
Sparse Core Ops, SparseCore 0:
  107.3 155.1 reduce-scatter.2
  417.2 128.3 reduce-scatter.4
where the time goes:
time: 621 us; the launch traced here: 619 us
  waiting for transfers between devices  421 us (68%)
  blocking collectives  121 us (19%)
  other arithmetic  26.1 us (4%)
  starting transfers between devices  19 us (3%)
  between operations  13.7 us (2%)
  local copies, waits for them, and re-layouts  12.3 us (2%)
    reduce_scatter x2, waiting for transfers between devices, sum_in_two_steps(): own = lax.psum_scatter(padded, axis, scatter_dimension=0, tiled=True)  284 us
    all_to_all x4, waiting for transfers between devices, copy_for_each(): return lax.all_to_all(copies, axis, split_axis=0, concat_axis=0, tiled=True)  137 us
    all_gather x2, blocking collectives, sum_in_two_steps(): whole = lax.all_gather(own, axis, axis=0, tiled=True)  111 us
    reduce_sum x5, other arithmetic, taken_together(): return copy_for_each(array, axis).sum(axis=0)  19.4 us
    all_to_all x4, starting transfers between devices, copy_for_each(): return lax.all_to_all(copies, axis, split_axis=0, concat_axis=0, tiled=True)  18.9 us
  transfers between devices with their start and end apart: 6, of which 5 were waited for; matrix products, arithmetic and copies ran while one was open for 1% of the time, Pallas kernels for 0%

commit v1 on v0

v1 whole, which is shorter than its diff:
```python
import functools

import jax
import jax.numpy as jnp
from jax import lax
from jax.experimental import pallas as pl
from jax.experimental.pallas import tpu as pltpu
from jax.sharding import PartitionSpec as P

epsilon = 1e-06
residual_weight = 0.5
MESH = pl.DeviceIdType.MESH
f32 = jnp.float32
bf16 = jnp.bfloat16


def in_three(column):
    hi = column.astype(bf16).astype(f32)
    mid = (column - hi).astype(bf16).astype(f32)
    lo = (column - hi - mid).astype(bf16).astype(f32)
    return hi, mid, lo


def with_lanes(tile, at, columns):
    lane = lax.broadcasted_iota(jnp.int32, tile.shape, 1)
    for k, column in enumerate(columns):
        tile = jnp.where(lane == at + k, column, tile)
    return tile


def kernel(
    dims,
    tok,
    gains,
    gate_w,
    value_w,
    gate_scale,
    value_scale,
    conv_gate,
    conv_value,
    down_w,
    down_scale,
    out,
    raw_in,
    raw_down,
    w_in,
    w_down,
    part,
    part_halo,
    got,
    got_halo,
    pre,
    hid,
    down_part,
    win,
    sums,
    cur,
    norm,
    w_sem,
    ps,
    pr,
    qs,
    qr,
    gs,
    gr,
    zs,
    zr,
    ms,
    mr,
    bs,
    br,
    ns,
    nr,
):
    layers, nz, nc, width, ff, ffp, blk, taps = dims
    owners = nz // nc
    half = nc // 2
    halo = taps - 1
    model_width = width * nc
    z = lax.axis_index("ra")
    c = lax.axis_index("cb")
    mine = lax.rem(z, nc)
    rank = z // nc

    def along_z(d):
        return {"ra": lax.rem(z + d + 2 * nz, nz), "cb": c}

    def along_c(k):
        return {"ra": z, "cb": lax.rem(c + k, nc)}

    def send(src, dst, ssem, rsem, to):
        return pltpu.make_async_remote_copy(
            src_ref=src, dst_ref=dst, send_sem=ssem, recv_sem=rsem, device_id=to, device_id_type=MESH
        )

    loads = []
    for layer in range(layers):
        for k, (src, dst) in enumerate(
            ((gate_w, raw_in.at[layer, 0]), (value_w, raw_in.at[layer, 1]), (down_w, raw_down.at[layer]))
        ):
            load = pltpu.make_async_copy(src.at[layer], dst, w_sem.at[layer, k])
            load.start()
            loads.append(load)

    barrier = pltpu.get_barrier_semaphore()
    peers = [along_c(k) for k in range(1, nc)]
    peers += [along_z(d) for d in range(-half, half + 1) if d != 0]
    peers += [along_z(nc * j) for j in range(1, owners)]
    for to in peers:
        pl.semaphore_signal(barrier, inc=1, device_id=to, device_id_type=MESH)

    edge = ff // 128 * 128
    for layer in range(layers):
        for s in range(2):
            w_in[layer, :, s * ffp + edge : (s + 1) * ffp] = jnp.zeros((width, ffp - edge), bf16)
        w_down[layer, ff:, :] = jnp.zeros((ffp - ff, width), bf16)
        part_halo[layer, 0] = jnp.zeros((halo, 2 * ffp), bf16)
        hid[layer, c, :, edge:] = jnp.zeros((blk, ffp - edge), bf16)

    def take_weights(layer):
        for load in loads[3 * layer : 3 * layer + 3]:
            load.wait()
        w_in[layer, :, 0:ff] = raw_in[layer, 0].astype(bf16)
        w_in[layer, :, ffp : ffp + ff] = raw_in[layer, 1].astype(bf16)
        w_down[layer, 0:ff, :] = raw_down[layer].astype(bf16)

    def partials(x, layer):
        scaled = (x * gains[layer : layer + 1, :]).astype(bf16)
        p = jnp.dot(scaled, w_in[layer], preferred_element_type=f32)
        squares = in_three(jnp.sum(x * x, axis=1, keepdims=True))
        last = with_lanes(p[:, edge:ffp], ff - edge, squares)
        return jnp.concatenate([p[:, :edge], last, p[:, ffp:]], axis=1)

    def part_copy(layer, b, src):
        return send(part.at[layer, b], got.at[layer, src], ps.at[layer, b], pr.at[layer, src], {"ra": z, "cb": b})

    def halo_copy(layer, b, src):
        return send(
            part_halo.at[layer, b], got_halo.at[layer, src], qs.at[layer, b], qr.at[layer, src], {"ra": z, "cb": b}
        )

    def hid_copy(layer, b, to):
        return send(
            hid.at[layer, b], hid.at[layer, b], gs.at[layer, to], gr.at[layer, b], {"ra": z, "cb": to}
        )

    def win_copy(layer, b, slot):
        return send(
            down_part.at[layer, b], win.at[layer, slot], zs.at[layer, b], zr.at[layer, slot], along_z(slot - (half - 1))
        )

    def sum_copy(layer, k, j):
        return send(sums.at[layer, k], sums.at[layer, k], ms.at[layer, j], mr.at[layer, k], along_z(nc * j))

    def cur_copy(layer, b, slot):
        return send(
            cur.at[layer, b], cur.at[layer, b], bs.at[layer, slot], br.at[layer, slot], along_z(half - 1 - slot)
        )

    def norm_copy(b, to):
        return send(norm.at[b], norm.at[b], ns.at[to], nr.at[b], {"ra": z, "cb": to})

    def near_first(i):
        return (2 * lax.rem(i, 2) - 1) * ((i + 1) // 2)

    for layer in range(layers):
        take_weights(layer) if layer == 0 else None
        if layer == 0:
            p = partials(tok[...].astype(f32), 0).reshape(nc, blk, 2 * ffp)
            part[0] = p.astype(bf16)
            for b in range(1, nc):
                part_halo[0, b] = p[b - 1, blk - halo :, :].astype(bf16)
            pl.semaphore_wait(barrier, len(peers))
            for k in (4, 3, 5, 2, 6, 1, 7) if nc == 8 else range(1, nc):
                to = lax.rem(c + k, nc)
                part_copy(0, to, c).start()
                halo_copy(0, to, c).start()
        else:

            def one_block(i, carry, layer=layer):
                d = near_first(i)
                b = lax.rem(z + d + nz, nc)
                slot = d + (half - 1)

                @pl.when(i > 0)
                def _():
                    cur_copy(layer - 1, b, slot).wait_recv()

                p = partials(cur[layer - 1, b].astype(f32), layer)
                part[layer, b] = p.astype(bf16)

                @pl.when(b != c)
                def _():
                    part_copy(layer, b, c).start()

                after = lax.rem(b + 1, nc)

                @pl.when(after != 0)
                def _():
                    part_halo[layer, after] = p[blk - halo :, :].astype(bf16)

                @pl.when(after != c)
                def _():
                    halo_copy(layer, after, c).start()

                return carry

            lax.fori_loop(0, nc, one_block, 0)

        got[layer, c] = part[layer, c]
        got_halo[layer, c] = part_halo[layer, c]
        if layer + 1 < layers:
            take_weights(layer + 1)
        for k in range(1, nc):
            src = lax.rem(c + k, nc)
            part_copy(layer, c, src).wait_recv()
            halo_copy(layer, c, src).wait_recv()
        for buf, rows, at in ((got_halo, halo, 8 - halo), (got, blk, 8)):
            total = buf[layer, 0].astype(f32)
            for src in range(1, nc):
                total = total + buf[layer, src].astype(f32)
            squares = jnp.sum(total[:, ff : ff + 3], axis=1, keepdims=True)
            inverse = lax.rsqrt(squares / model_width + epsilon)
            pre[at : at + rows, 0:ff] = inverse * gate_scale[layer : layer + 1, :] * total[:, 0:ff]
            pre[at : at + rows, ffp : ffp + ff] = (
                inverse * value_scale[layer : layer + 1, :] * total[:, ffp : ffp + ff]
            )
        convs = []
        for lane, weights in ((0, conv_gate), (ffp, conv_value)):
            y = None
            for k in range(taps):
                term = pre[8 - halo + k : 8 - halo + k + blk, lane : lane + ff] * weights[layer, k : k + 1, :]
                y = term if y is None else y + term
            convs.append(y)
        hid[layer, c, :, 0:ff] = (jax.nn.gelu(convs[0], approximate=True) * convs[1]).astype(bf16)
        for k in (4, 3, 5, 2, 6, 1, 7) if nc == 8 else range(1, nc):
            hid_copy(layer, c, lax.rem(c + k, nc)).start()

        def down_block(i, carry, layer=layer):
            b = lax.rem(c + near_first(i) + nc, nc)

            @pl.when(i > 0)
            def _():
                hid_copy(layer, b, c).wait_recv()

            down_part[layer, b] = jnp.dot(hid[layer, b], w_down[layer], preferred_element_type=f32).astype(bf16)
            slot = lax.rem(b - z + (half - 1) + nz, nc)

            @pl.when(slot != half - 1)
            def _():
                win_copy(layer, b, slot).start()

            return carry

        lax.fori_loop(0, nc, down_block, 0)

        win[layer, half - 1] = down_part[layer, mine]
        for slot in range(nc):
            if slot != half - 1:
                win_copy(layer, mine, slot).wait_recv()
        total = win[layer, 0].astype(f32)
        for slot in range(1, nc):
            total = total + win[layer, slot].astype(f32)
        sums[layer, rank] = total.astype(bf16)
        far_first = sorted(range(1, owners), key=lambda j: -min(j, owners - j))
        for j in far_first:
            sum_copy(layer, rank, j).start()
        for j in far_first:
            sum_copy(layer, lax.rem(rank + j, owners), j).wait_recv()
        total = sums[layer, 0].astype(f32)
        for k in range(1, owners):
            total = total + sums[layer, k].astype(f32)
        if layer == 0:
            own = tok[pl.ds(pl.multiple_of(mine * blk, blk), blk), :].astype(f32)
        else:
            own = cur[layer - 1, mine].astype(f32)
        new = (residual_weight * own + down_scale[layer : layer + 1, :] * total).astype(bf16)

        if layer == layers - 1:
            wide = new.astype(f32)
            squares = in_three(jnp.sum(wide * wide, axis=1, keepdims=True))
            norm[c] = with_lanes(jnp.zeros((blk, 128), f32), 0, squares).astype(bf16)
            for k in range(1, nc):
                norm_copy(c, lax.rem(c + k, nc)).start()
            for k in range(1, nc):
                norm_copy(lax.rem(c + k, nc), c).wait_recv()
            both = norm[0].astype(f32)
            for k in range(1, nc):
                both = both + norm[k].astype(f32)
            squares = jnp.sum(both[:, 0:3], axis=1, keepdims=True)
            inverse = lax.rsqrt(squares / model_width + epsilon)
            new = (wide * inverse * gains[layers : layers + 1, :]).astype(bf16)
        cur[layer, mine] = new
        for slot in range(nc):
            if slot != half - 1:
                cur_copy(layer, mine, slot).start()

    last = layers - 1

    def put_block(i, carry):
        d = near_first(i)
        b = lax.rem(z + d + nz, nc)

        @pl.when(i > 0)
        def _():
            cur_copy(last, b, d + (half - 1)).wait_recv()

        out[pl.ds(pl.multiple_of(b * blk, blk), blk), :] = cur[last, b]
        return carry

    lax.fori_loop(0, nc, put_block, 0)

    for layer in range(layers):
        for k in range(1, nc):
            to = lax.rem(c + k, nc)
            part_copy(layer, to, c).wait_send()
            halo_copy(layer, to, c).wait_send()
            hid_copy(layer, c, to).wait_send()
        for slot in range(nc):
            if slot != half - 1:
                win_copy(layer, lax.rem(z + slot - (half - 1) + nz, nc), slot).wait_send()
                cur_copy(layer, mine, slot).wait_send()
        for j in range(1, owners):
            sum_copy(layer, rank, j).wait_send()
    for k in range(1, nc):
        norm_copy(c, lax.rem(c + k, nc)).wait_send()


def on_device(
    tokens,
    norm_gains,
    gate_weight,
    value_weight,
    gate_scale,
    value_scale,
    conv_gate,
    conv_value,
    down_weight,
    down_scale,
):
    nz, nc = lax.axis_size("ra"), lax.axis_size("cb")
    rows, width = tokens.shape
    layers, _, ff = gate_weight.shape
    taps = conv_gate.shape[1]
    ffp = (ff + 3 + 127) // 128 * 128
    blk = rows // nc
    owners = nz // nc
    dims = (layers, nz, nc, width, ff, ffp, blk, taps)
    vmem = pl.BlockSpec(memory_space=pltpu.VMEM)
    hbm = pl.BlockSpec(memory_space=pl.ANY)
    dma = pltpu.SemaphoreType.DMA
    return pl.pallas_call(
        functools.partial(kernel, dims),
        out_shape=jax.ShapeDtypeStruct((rows, width), bf16),
        in_specs=[vmem, vmem, hbm, hbm, vmem, vmem, vmem, vmem, hbm, vmem],
        out_specs=vmem,
        scratch_shapes=[
            pltpu.VMEM((layers, 2, width, ff), f32),
            pltpu.VMEM((layers, ff, width), f32),
            pltpu.VMEM((layers, width, 2 * ffp), bf16),
            pltpu.VMEM((layers, ffp, width), bf16),
            pltpu.VMEM((layers, nc, blk, 2 * ffp), bf16),
            pltpu.VMEM((layers, nc, taps - 1, 2 * ffp), bf16),
            pltpu.VMEM((layers, nc, blk, 2 * ffp), bf16),
            pltpu.VMEM((layers, nc, taps - 1, 2 * ffp), bf16),
            pltpu.VMEM((8 + blk, 2 * ffp), f32),
            pltpu.VMEM((layers, nc, blk, ffp), bf16),
            pltpu.VMEM((layers, nc, blk, width), bf16),
            pltpu.VMEM((layers, nc, blk, width), bf16),
            pltpu.VMEM((layers, owners, blk, width), bf16),
            pltpu.VMEM((layers, nc, blk, width), bf16),
            pltpu.VMEM((nc, blk, 128), bf16),
            dma((layers, 3)),
        ]
        + [dma((layers, nc))] * 8
        + [dma((layers, owners))] * 2
        + [dma((layers, nc))] * 2
        + [dma((nc,))] * 2,
        compiler_params=pltpu.CompilerParams(
            collective_id=0, has_side_effects=True, vmem_limit_bytes=40 * 2**20
        ),
        cost_estimate=pl.CostEstimate(flops=4 * 10**8, bytes_accessed=10**7, transcendentals=0),
    )(
        tokens,
        norm_gains,
        gate_weight,
        value_weight,
        gate_scale,
        value_scale,
        conv_gate,
        conv_value,
        down_weight,
        down_scale,
    )


def solution(mesh):
    in_specs = (
        P("grp", "cb"),
        P(None, "cb"),
        P(None, "cb", "ra"),
        P(None, "cb", "ra"),
        P(None, "ra"),
        P(None, "ra"),
        P(None, None, "ra"),
        P(None, None, "ra"),
        P(None, "ra", "cb"),
        P(None, "cb"),
    )
    out_specs = P("grp", "cb")
    return jax.shard_map(on_device, mesh=mesh, in_specs=in_specs, out_specs=out_specs, check_vma=False)
```

time: 621 us -> 161 us (0.26)
  waiting for transfers between devices: 421 us -> 0 us
  Pallas kernels: 0 us -> 154 us
  blocking collectives: 121 us -> 0 us
  other arithmetic: 26.1 us -> 0 us
  starting transfers between devices: 19 us -> 0 us
  between operations: 13.7 us -> 0.11 us
    reduce_scatter x2 -> x0, waiting for transfers between devices: 284 us -> none  [sum_in_two_steps(): own = lax.psum_scatter(padded, axis, scatter_dimension=0, tiled=True)]
    pallas_call x0 -> x1, Pallas kernels: none -> 154 us  [on_device(): pl.pallas_call(functools.partial(kernel, dims), out_shape=jax.ShapeDtypeS...]
    all_to_all x4 -> x0, waiting for transfers between devices: 137 us -> none  [copy_for_each(): return lax.all_to_all(copies, axis, split_axis=0, concat_axis=0, tiled=True)]
    all_gather x2 -> x0, blocking collectives: 111 us -> none  [sum_in_two_steps(): whole = lax.all_gather(own, axis, axis=0, tiled=True)]
    reduce_sum x8 -> x0, other arithmetic: 21 us -> none  [the longest x5 19.4 us: taken_together(): return copy_for_each(array, axis).sum(axis=0)]
    all_to_all x4 -> x0, starting transfers between devices: 18.9 us -> none  [copy_for_each(): return lax.all_to_all(copies, axis, split_axis=0, concat_axis=0, tiled=True)]
    all_to_all x1 -> x0, blocking collectives: 9.39 us -> none  [copy_for_each(): return lax.all_to_all(copies, axis, split_axis=0, concat_axis=0, tiled=True)]
    broadcast_in_dim x5 -> x0, local copies, waits for them, and re-layouts: 9.11 us -> none  [copy_for_each(): copies = jnp.broadcast_to(array, (lax.axis_size(axis), *array.shape))]
  transfers between devices with their start and end apart: 6 -> 0, of which waited for: 5 -> 0; matrix products, arithmetic and copies ran while one was open for 1% -> 0% of each run, Pallas kernels for 0% -> 0%
where the time goes in v1:
time: 161 us
  Pallas kernels  154 us (96%)
  local copies, waits for them, and re-layouts  7.24 us (4%)
    pallas_call x1, Pallas kernels, on_device(): pl.pallas_call(functools.partial(kernel, dims), out_shape=jax.ShapeDtypeS...  154 us
    unnamed x17, local copies, waits for them, and re-layouts  7.24 us

profile of v1, /device:TPU:40, one launch (start us, length us, event | category | flops | bytes accessed | tf_op | source)
XLA Modules:
  0.0 161.1 jit_solution(16311577812133228913)
XLA Ops:
  0.0 0.7 copy.13.conv_gate
  0.7 0.7 copy.14.conv_value
  1.4 1.8 %copy.11.gate_w = f32[2,512,352]{2,1,0:T(8,128)S(1)} copy(f32[2,512,352]{1,2,0:T(8,128)} %param.12) | data formatting | bytes 2883584 | tf_op args[2]
  3.2 0.0 copy-start.1
  3.3 0.0 copy-start.2
  3.3 0.0 copy-start.3
  3.3 0.0 copy-start.4
  3.3 0.0 copy-start.5
  3.3 1.9 %copy.12.value_w = f32[2,512,352]{2,1,0:T(8,128)S(1)} copy(f32[2,512,352]{1,2,0:T(8,128)} %param.13) | data formatting | bytes 2883584 | tf_op args[3]
  5.2 0.0 copy-done.1
  5.2 0.0 copy-done.2
  5.2 0.0 copy-done.3
  5.2 0.0 copy-done.4
  5.3 0.0 copy-done.5
  5.3 0.0 copy-start
  5.3 1.4 copy-done
  6.6 153.7 %shard_map.100 = bf16[256,512]{1,0:T(8,128)(2,1)S(1)} custom-call(bf16[256,512]{1,0:T(8,128)(2,1)S(1)} %copy-done.1, f32[3,512]{1,0:T(4,128)S(1)} %copy-done.2, f32[2,512,352]{2,1,0:T(8,128)S(1)} %copy.11.gate_w, f32[2,512,352]{2,1,0:T(8,128)S(1)} %copy.12.value_w, f32[2,352]{1,0:T(2,128)S(1)} %copy-done.4, f32[2,352]{1,0:T(2,128)S(1)} %copy-done.5, ...), custom_call_target="tpu_custom_call" | custom-call | flops 400000000 | bytes 10000000 | tf_op jit(solution)/shard_map/pallas_call | solution.py:352
  160.4 0.7 copy.16
Async XLA Ops:
  3.2 2.0 %copy-start.1 = (bf16[256,512]{1,0:T(8,128)(2,1)S(1)}, bf16[256,512]{1,0:T(8,128)(2,1)}, u32[]{:S(2)}) copy-start(bf16[256,512]{1,0:T(8,128)(2,1)} %tok.1) | copy-start | bytes 786436
  3.3 2.0 %copy-start.2 = (f32[3,512]{1,0:T(4,128)S(1)}, f32[3,512]{1,0:T(4,128)}, u32[]{:S(2)}) copy-start(f32[3,512]{1,0:T(4,128)} %gains.1) | copy-start | bytes 18436
  3.3 2.0 %copy-start.3 = (f32[2,512]{1,0:T(2,128)S(1)}, f32[2,512]{1,0:T(2,128)}, u32[]{:S(2)}) copy-start(f32[2,512]{1,0:T(2,128)} %down_scale.1) | copy-start | bytes 12292
  3.3 2.0 %copy-start.4 = (f32[2,352]{1,0:T(2,128)S(1)}, f32[2,352]{1,0:T(2,128)}, u32[]{:S(2)}) copy-start(f32[2,352]{1,0:T(2,128)} %gate_scale.1) | copy-start | bytes 8452
  3.3 2.0 %copy-start.5 = (f32[2,352]{1,0:T(2,128)S(1)}, f32[2,352]{1,0:T(2,128)}, u32[]{:S(2)}) copy-start(f32[2,352]{1,0:T(2,128)} %value_scale.1) | copy-start | bytes 8452
  5.3 1.4 copy-start

commit v2 on v1

v2 whole, which is shorter than its diff:
```python
import functools

import jax
import jax.numpy as jnp
from jax import lax
from jax.experimental import pallas as pl
from jax.experimental.pallas import tpu as pltpu
from jax.sharding import PartitionSpec as P

epsilon = 1e-06
residual_weight = 0.5
MESH = pl.DeviceIdType.MESH
f32 = jnp.float32
bf16 = jnp.bfloat16


def in_three(column):
    hi = column.astype(bf16).astype(f32)
    mid = (column - hi).astype(bf16).astype(f32)
    lo = (column - hi - mid).astype(bf16).astype(f32)
    return hi, mid, lo


def with_lanes(tile, at, columns):
    lane = lax.broadcasted_iota(jnp.int32, tile.shape, 1)
    for k, column in enumerate(columns):
        tile = jnp.where(lane == at + k, column, tile)
    return tile


def as_row(column):
    n = column.shape[0]
    at = lax.broadcasted_iota(jnp.int32, (n, 128), 0) == lax.broadcasted_iota(jnp.int32, (n, 128), 1)
    return jnp.sum(jnp.where(at, column, 0.0), axis=0, keepdims=True)


def as_column(row, n, first):
    at = lax.broadcasted_iota(jnp.int32, (n, 128), 0) + first == lax.broadcasted_iota(jnp.int32, (n, 128), 1)
    return jnp.sum(jnp.where(at, row, 0.0), axis=1, keepdims=True)


def kernel(
    dims,
    tok_hbm,
    gains_hbm,
    gate_w,
    value_w,
    gate_scale_hbm,
    value_scale_hbm,
    conv_gate_hbm,
    conv_value_hbm,
    down_w,
    down_scale_hbm,
    out,
    tok,
    gains,
    gate_scale,
    value_scale,
    conv_gate,
    conv_value,
    down_scale,
    raw_in,
    raw_down,
    w_first,
    w_later,
    w_down,
    part,
    part_halo,
    got,
    got_halo,
    pre,
    hid,
    down_part,
    win,
    sums,
    cur,
    squares_row,
    inverse_row,
    small_sem,
    w_sem,
    ps,
    pr,
    qs,
    qr,
    gs,
    gr,
    zs,
    zr,
    ms,
    mr,
    bs,
    br,
    ns,
    nr,
    vs,
    vr,
    greeting,
):
    layers, nz, nc, width, ff, ffp, blk, taps = dims
    owners = nz // nc
    half = nc // 2
    rows = blk // 2
    halo = taps - 1
    model_width = width * nc
    z = lax.axis_index("ra")
    c = lax.axis_index("cb")
    mine = lax.rem(z, nc)
    rank = z // nc

    def along_z(d):
        return {"ra": lax.rem(z + d + 2 * nz, nz), "cb": c}

    def along_c(k):
        return {"ra": z, "cb": lax.rem(c + k, nc)}

    def send(src, dst, ssem, rsem, to):
        return pltpu.make_async_remote_copy(
            src_ref=src, dst_ref=dst, send_sem=ssem, recv_sem=rsem, device_id=to, device_id_type=MESH
        )

    barrier = pltpu.get_barrier_semaphore()
    peers = [along_c(k) for k in range(1, nc)] + [along_z(1), along_z(-1)]
    for to in peers:
        pl.semaphore_signal(barrier, inc=1, device_id=to, device_id_type=MESH)

    def greet(stage):
        for d in (-(2**stage), 2**stage):
            pl.semaphore_signal(greeting.at[stage], inc=1, device_id=along_z(d), device_id_type=MESH)

    def greeted(stage):
        pl.semaphore_wait(greeting.at[stage], 2)

    def weight_loads(layer):
        for k, (src, dst) in enumerate(
            (
                (gate_w, raw_in.at[layer, 0, pl.ds(0, ff)]),
                (value_w, raw_in.at[layer, 1, pl.ds(0, ff)]),
                (down_w, raw_down.at[layer]),
            )
        ):
            yield pltpu.make_async_copy(src.at[layer], dst, w_sem.at[layer, k])

    small = [
        pltpu.make_async_copy(src, dst, small_sem.at[k])
        for k, (src, dst) in enumerate(
            (
                (tok_hbm, tok),
                (gains_hbm, gains),
                (gate_scale_hbm, gate_scale),
                (value_scale_hbm, value_scale),
                (conv_gate_hbm, conv_gate),
                (conv_value_hbm, conv_value),
                (down_scale_hbm, down_scale),
            )
        )
    ]
    weights = [list(weight_loads(layer)) for layer in range(layers)]
    for load in small[:2] + weights[0] + small[2:] + sum(weights[1:], []):
        load.start()

    edge = ff // 128 * 128
    for layer in range(layers):
        for s in range(2):
            raw_in[layer, s, ff:, :] = jnp.zeros((ffp - ff, width), f32)
        w_down[layer, ff:, :] = jnp.zeros((ffp - ff, width), bf16)
        part_halo[layer, 0] = jnp.zeros((halo, 2 * ffp), bf16)
        hid[layer, c, :, edge:] = jnp.zeros((blk, ffp - edge), bf16)

    def take_in(layer):
        for s in range(2):
            weights[layer][s].wait()
            if layer == 0:
                w_first[s * ffp : (s + 1) * ffp, :] = raw_in[0, s].astype(bf16)
            else:
                w_later[layer - 1, :, s * ffp : (s + 1) * ffp] = raw_in[layer, s].T.astype(bf16)

    def take_down(layer):
        weights[layer][2].wait()
        w_down[layer, 0:ff, :] = raw_down[layer].astype(bf16)

    def partials(x, layer):
        scaled = (x * gains[layer : layer + 1, :]).astype(bf16)
        if layer == 0:
            p = lax.dot_general(scaled, w_first[...], (((1,), (1,)), ((), ())), preferred_element_type=f32)
        else:
            p = jnp.dot(scaled, w_later[layer - 1], preferred_element_type=f32)
        squares = in_three(jnp.sum(x * x, axis=1, keepdims=True))
        last = with_lanes(p[:, edge:ffp], ff - edge, squares)
        return jnp.concatenate([p[:, :edge], last, p[:, ffp:]], axis=1)

    def part_copy(layer, b, src):
        return send(part.at[layer, b], got.at[layer, src], ps.at[layer, b], pr.at[layer, src], {"ra": z, "cb": b})

    def halo_copy(layer, b, src):
        return send(
            part_halo.at[layer, b], got_halo.at[layer, src], qs.at[layer, b], qr.at[layer, src], {"ra": z, "cb": b}
        )

    def hid_copy(layer, b, to):
        return send(hid.at[layer, b], hid.at[layer, b], gs.at[layer, to], gr.at[layer, b], {"ra": z, "cb": to})

    def away(p, slot):
        return slot - (half - 1) - p

    def slot_of(p, b):
        return lax.rem(b - z + (half - 1) + p + nz, nc)

    def others(p):
        return sorted((s for s in range(nc) if away(p, s) != 0), key=lambda s: -abs(away(p, s)))

    def win_copy(layer, p, b, slot):
        return send(
            down_part.at[layer, b, p],
            win.at[layer, p, slot],
            zs.at[layer, p, b],
            zr.at[layer, p, slot],
            along_z(away(p, slot)),
        )

    def sum_copy(layer, p, k, j):
        return send(
            sums.at[layer, p, k], sums.at[layer, p, k], ms.at[layer, p, j], mr.at[layer, p, k], along_z(nc * j)
        )

    def cur_copy(layer, p, b, slot):
        return send(
            cur.at[layer, b, p],
            cur.at[layer, b, p],
            bs.at[layer, p, slot],
            br.at[layer, p, slot],
            along_z(-away(p, slot)),
        )

    def squares_copy(src, to):
        return send(squares_row.at[src], squares_row.at[src], ns.at[to], nr.at[src], {"ra": z, "cb": to})

    def inverse_copy(p, b, slot):
        return send(
            inverse_row.at[b, p], inverse_row.at[b, p], vs.at[p, slot], vr.at[p, slot], along_z(-away(p, slot))
        )

    def near_first(i):
        return (2 * lax.rem(i, 2) - 1) * ((i + 1) // 2)

    far_c = sorted(range(1, nc), key=lambda k: -min(k, nc - k))
    far_owner = sorted(range(1, owners), key=lambda j: -min(j, owners - j))

    for layer in range(layers):
        if layer == 0:
            small[0].wait()
            small[1].wait()
            take_in(0)
            p = partials(tok[...].astype(f32), 0).reshape(nc, blk, 2 * ffp)
            part[0] = p.astype(bf16)
            for b in range(1, nc):
                part_halo[0, b] = p[b - 1, blk - halo :, :].astype(bf16)
            pl.semaphore_wait(barrier, len(peers))
            for k in far_c:
                to = lax.rem(c + k, nc)
                part_copy(0, to, c).start()
                halo_copy(0, to, c).start()
            greet(0)
        else:

            def one_block(i, carry, layer=layer):
                b = lax.rem(z + near_first(i) + nz, nc)

                @pl.when(i > 0)
                def _():
                    for p in range(2):
                        cur_copy(layer - 1, p, b, slot_of(p, b)).wait_recv()

                p = partials(cur[layer - 1, b].reshape(blk, width).astype(f32), layer)
                part[layer, b] = p.astype(bf16)

                @pl.when(b != c)
                def _():
                    part_copy(layer, b, c).start()

                after = lax.rem(b + 1, nc)

                @pl.when(after != 0)
                def _():
                    part_halo[layer, after] = p[blk - halo :, :].astype(bf16)

                @pl.when(after != c)
                def _():
                    halo_copy(layer, after, c).start()

                return carry

            lax.fori_loop(0, nc, one_block, 0)

        got[layer, c] = part[layer, c]
        got_halo[layer, c] = part_halo[layer, c]
        if layer == 0:
            take_down(0)
            greeted(0)
            greet(1)
            for load in small[2:]:
                load.wait()
        for k in range(1, nc):
            src = lax.rem(c + k, nc)
            part_copy(layer, c, src).wait_recv()
            halo_copy(layer, c, src).wait_recv()
        for buf, count, at in ((got_halo, halo, 8 - halo), (got, blk, 8)):
            total = buf[layer, 0].astype(f32)
            for src in range(1, nc):
                total = total + buf[layer, src].astype(f32)
            squares = jnp.sum(total[:, ff : ff + 3], axis=1, keepdims=True)
            inverse = lax.rsqrt(squares / model_width + epsilon)
            pre[at : at + count, 0:ff] = inverse * gate_scale[layer : layer + 1, :] * total[:, 0:ff]
            pre[at : at + count, ffp : ffp + ff] = (
                inverse * value_scale[layer : layer + 1, :] * total[:, ffp : ffp + ff]
            )
        convs = []
        for lane, tap_weights in ((0, conv_gate), (ffp, conv_value)):
            y = None
            for k in range(taps):
                term = pre[8 - halo + k : 8 - halo + k + blk, lane : lane + ff] * tap_weights[k, layer : layer + 1, :]
                y = term if y is None else y + term
            convs.append(y)
        hid[layer, c, :, 0:ff] = (jax.nn.gelu(convs[0], approximate=True) * convs[1]).astype(bf16)
        for k in far_c:
            hid_copy(layer, c, lax.rem(c + k, nc)).start()
        if layer == 0:
            greeted(1)
            greet(2)

        def down_block(i, carry, layer=layer):
            b = lax.rem(c + near_first(i) + nc, nc)

            @pl.when(i > 0)
            def _():
                hid_copy(layer, b, c).wait_recv()

            d = jnp.dot(hid[layer, b], w_down[layer], preferred_element_type=f32)
            down_part[layer, b] = d.astype(bf16).reshape(2, rows, width)
            slot = slot_of(0, b)

            @pl.when(slot != half - 1)
            def _():
                win_copy(layer, 0, b, slot).start()

            return carry

        lax.fori_loop(0, nc, down_block, 0)
        for slot in others(1):
            win_copy(layer, 1, lax.rem(z + away(1, slot) + nz, nc), slot).start()
        if layer + 1 < layers:
            take_in(layer + 1)
            take_down(layer + 1)
        if layer == 0:
            greeted(2)
            greet(3)

        for p in range(2):
            win[layer, p, half - 1 + p] = down_part[layer, mine, p]
            for slot in others(p):
                win_copy(layer, p, mine, slot).wait_recv()
            total = win[layer, p, 0].astype(f32)
            for slot in range(1, nc):
                total = total + win[layer, p, slot].astype(f32)
            sums[layer, p, rank] = total.astype(bf16)
            if layer == 0 and p == 0:
                greeted(3)
            for j in far_owner:
                sum_copy(layer, p, rank, j).start()
        lengths = []
        for p in range(2):
            for j in far_owner:
                sum_copy(layer, p, lax.rem(rank + j, owners), j).wait_recv()
            total = sums[layer, p, 0].astype(f32)
            for k in range(1, owners):
                total = total + sums[layer, p, k].astype(f32)
            if layer == 0:
                own = tok[pl.ds(pl.multiple_of(mine * blk + p * rows, rows), rows), :].astype(f32)
            else:
                own = cur[layer - 1, mine, p].astype(f32)
            new = (residual_weight * own + down_scale[layer : layer + 1, :] * total).astype(bf16)
            cur[layer, mine, p] = new
            for slot in others(p):
                cur_copy(layer, p, mine, slot).start()
            if layer == layers - 1:
                wide = new.astype(f32)
                lengths.append(jnp.sum(wide * wide, axis=1, keepdims=True))

    squares_row[c] = as_row(jnp.concatenate(lengths, axis=0))
    for k in far_c:
        squares_copy(c, lax.rem(c + k, nc)).start()
    for k in range(1, nc):
        squares_copy(lax.rem(c + k, nc), c).wait_recv()
    total = squares_row[0]
    for k in range(1, nc):
        total = total + squares_row[k]
    inverse = lax.rsqrt(total / model_width + epsilon)
    for p in range(2):
        inverse_row[mine, p] = inverse
    for p in range(2):
        for slot in others(p):
            inverse_copy(p, mine, slot).start()

    last = layers - 1

    def put_block(i, carry):
        b = lax.rem(z + near_first(i) + nz, nc)

        @pl.when(i > 0)
        def _():
            for p in range(2):
                cur_copy(last, p, b, slot_of(p, b)).wait_recv()
                inverse_copy(p, b, slot_of(p, b)).wait_recv()

        for p in range(2):
            scale = as_column(inverse_row[b, p], rows, p * rows)
            wide = cur[last, b, p].astype(f32) * scale * gains[layers : layers + 1, :]
            out[pl.ds(pl.multiple_of(b * blk + p * rows, rows), rows), :] = wide.astype(bf16)
        return carry

    lax.fori_loop(0, nc, put_block, 0)

    for layer in range(layers):
        for k in range(1, nc):
            to = lax.rem(c + k, nc)
            part_copy(layer, to, c).wait_send()
            halo_copy(layer, to, c).wait_send()
            hid_copy(layer, c, to).wait_send()
        for p in range(2):
            for slot in others(p):
                win_copy(layer, p, lax.rem(z + away(p, slot) + nz, nc), slot).wait_send()
                cur_copy(layer, p, mine, slot).wait_send()
            for j in range(1, owners):
                sum_copy(layer, p, rank, j).wait_send()
    for k in range(1, nc):
        squares_copy(c, lax.rem(c + k, nc)).wait_send()
    for p in range(2):
        for slot in others(p):
            inverse_copy(p, mine, slot).wait_send()


def on_device(
    tokens,
    norm_gains,
    gate_weight,
    value_weight,
    gate_scale,
    value_scale,
    conv_gate,
    conv_value,
    down_weight,
    down_scale,
):
    nz, nc = lax.axis_size("ra"), lax.axis_size("cb")
    rows, width = tokens.shape
    layers, _, ff = gate_weight.shape
    taps = conv_gate.shape[1]
    ffp = (ff + 3 + 127) // 128 * 128
    blk = rows // nc
    owners = nz // nc
    dims = (layers, nz, nc, width, ff, ffp, blk, taps)
    dma = pltpu.SemaphoreType.DMA
    operands = (
        tokens,
        norm_gains,
        gate_weight.swapaxes(1, 2),
        value_weight.swapaxes(1, 2),
        gate_scale,
        value_scale,
        conv_gate.swapaxes(0, 1),
        conv_value.swapaxes(0, 1),
        down_weight,
        down_scale,
    )
    small = [operands[k] for k in (0, 1, 4, 5, 6, 7, 9)]
    return pl.pallas_call(
        functools.partial(kernel, dims),
        out_shape=jax.ShapeDtypeStruct((rows, width), bf16),
        in_specs=[pl.BlockSpec(memory_space=pltpu.HBM)] * len(operands),
        out_specs=pl.BlockSpec(memory_space=pltpu.VMEM),
        scratch_shapes=[pltpu.VMEM(a.shape, a.dtype) for a in small]
        + [
            pltpu.VMEM((layers, 2, ffp, width), f32),
            pltpu.VMEM((layers, ff, width), f32),
            pltpu.VMEM((2 * ffp, width), bf16),
            pltpu.VMEM((layers - 1, width, 2 * ffp), bf16),
            pltpu.VMEM((layers, ffp, width), bf16),
            pltpu.VMEM((layers, nc, blk, 2 * ffp), bf16),
            pltpu.VMEM((layers, nc, taps - 1, 2 * ffp), bf16),
            pltpu.VMEM((layers, nc, blk, 2 * ffp), bf16),
            pltpu.VMEM((layers, nc, taps - 1, 2 * ffp), bf16),
            pltpu.VMEM((8 + blk, 2 * ffp), f32),
            pltpu.VMEM((layers, nc, blk, ffp), bf16),
            pltpu.VMEM((layers, nc, 2, blk // 2, width), bf16),
            pltpu.VMEM((layers, 2, nc, blk // 2, width), bf16),
            pltpu.VMEM((layers, 2, owners, blk // 2, width), bf16),
            pltpu.VMEM((layers, nc, 2, blk // 2, width), bf16),
            pltpu.VMEM((nc, 1, 128), f32),
            pltpu.VMEM((nc, 2, 1, 128), f32),
            dma((len(small),)),
            dma((layers, 3)),
        ]
        + [dma((layers, nc))] * 6
        + [dma((layers, 2, nc))] * 2
        + [dma((layers, 2, owners))] * 2
        + [dma((layers, 2, nc))] * 2
        + [dma((nc,))] * 2
        + [dma((2, nc))] * 2
        + [pltpu.SemaphoreType.REGULAR((4,))],
        compiler_params=pltpu.CompilerParams(
            collective_id=0, has_side_effects=True, vmem_limit_bytes=61 * 2**20
        ),
        cost_estimate=pl.CostEstimate(flops=4 * 10**8, bytes_accessed=10**7, transcendentals=0),
    )(*operands)


def solution(mesh):
    in_specs = (
        P("grp", "cb"),
        P(None, "cb"),
        P(None, "cb", "ra"),
        P(None, "cb", "ra"),
        P(None, "ra"),
        P(None, "ra"),
        P(None, None, "ra"),
        P(None, None, "ra"),
        P(None, "ra", "cb"),
        P(None, "cb"),
    )
    out_specs = P("grp", "cb")
    return jax.shard_map(on_device, mesh=mesh, in_specs=in_specs, out_specs=out_specs, check_vma=False)
```

time: 161 us -> 143 us (0.89)
  Pallas kernels: 154 us -> 141 us
  local copies, waits for them, and re-layouts: 7.24 us -> 1.67 us
    pallas_call x1, Pallas kernels: 154 us -> 141 us  [on_device(): pl.pallas_call(functools.partial(kernel, dims), out_shape=jax.ShapeDtypeS...]
    unnamed x17 -> x1, local copies, waits for them, and re-layouts: 7.24 us -> 1.67 us
where the time goes in v2:
time: 143 us; the launch traced here: 142 us
  Pallas kernels  141 us (99%)
  local copies, waits for them, and re-layouts  1.67 us (1%)
    pallas_call x1, Pallas kernels, on_device(): pl.pallas_call(functools.partial(kernel, dims), out_shape=jax.ShapeDtypeS...  141 us

profile of v2, /device:TPU:40, one launch (start us, length us, event | category | flops | bytes accessed | tf_op | source)
XLA Modules:
  0.0 142.4 jit_solution(18413066164864550298)
XLA Ops:
  0.0 140.7 %shard_map.100 = bf16[256,512]{1,0:T(8,128)(2,1)} custom-call(bf16[256,512]{1,0:T(8,128)(2,1)} %tok_hbm.1, f32[3,512]{1,0:T(4,128)} %gains_hbm.1, f32[2,352,512]{2,1,0:T(8,128)} %bitcast.4, f32[2,352,512]{2,1,0:T(8,128)} %bitcast.5, f32[2,352]{1,0:T(2,128)} %gate_scale_hbm.1, f32[2,352]{1,0:T(2,128)} %value_scale_hbm.1, f32[3,2,352]{2,1,0:T(2,128)} %bitcast.6, ...), custom_call_target="tpu_custom_call" | custom-call | flops 400000000 | bytes 10000000 | tf_op jit(solution)/shard_map/pallas_call | solution.py:475
  140.8 1.7 %copy.12 = bf16[256,512]{1,0:T(8,128)(2,1)} copy(bf16[256,512]{1,0:T(8,128)(2,1)} %shard_map.100) | data formatting | bytes 524288

commit v3 on v2

--- a/solution.py
+++ b/solution.py
@@ -76,6 +76,7 @@
     cur,
     squares_row,
     inverse_row,
+    result,
     small_sem,
     w_sem,
     ps,
@@ -94,6 +95,7 @@
     nr,
     vs,
     vr,
+    out_sem,
     greeting,
 ):
     layers, nz, nc, width, ff, ffp, blk, taps = dims
@@ -188,16 +190,25 @@
         last = with_lanes(p[:, edge:ffp], ff - edge, squares)
         return jnp.concatenate([p[:, :edge], last, p[:, ffp:]], axis=1)
 
+    most = pl.ds(0, nc - 1)
+
     def part_copy(layer, b, src):
-        return send(part.at[layer, b], got.at[layer, src], ps.at[layer, b], pr.at[layer, src], {"ra": z, "cb": b})
+        return send(part.at[layer, b], got.at[layer, src], ps.at[layer], pr.at[layer], {"ra": z, "cb": b})
+
+    def part_all(layer):
+        return send(part.at[layer, most], got.at[layer, most], ps.at[layer], pr.at[layer], along_c(1))
 
     def halo_copy(layer, b, src):
-        return send(
-            part_halo.at[layer, b], got_halo.at[layer, src], qs.at[layer, b], qr.at[layer, src], {"ra": z, "cb": b}
-        )
+        return send(part_halo.at[layer, b], got_halo.at[layer, src], qs.at[layer], qr.at[layer], {"ra": z, "cb": b})
+
+    def halo_all(layer):
+        return send(part_halo.at[layer, most], got_halo.at[layer, most], qs.at[layer], qr.at[layer], along_c(1))
 
     def hid_copy(layer, b, to):
-        return send(hid.at[layer, b], hid.at[layer, b], gs.at[layer, to], gr.at[layer, b], {"ra": z, "cb": to})
+        return send(hid.at[layer, b], hid.at[layer, b], gs.at[layer], gr.at[layer, b], {"ra": z, "cb": to})
+
+    def hid_all(layer):
+        return send(hid.at[layer, most], hid.at[layer, most], gs.at[layer], gr.at[layer, 0], along_c(1))
 
     def away(p, slot):
         return slot - (half - 1) - p
@@ -212,32 +223,57 @@
         return send(
             down_part.at[layer, b, p],
             win.at[layer, p, slot],
-            zs.at[layer, p, b],
-            zr.at[layer, p, slot],
+            zs.at[layer],
+            zr.at[layer, p],
             along_z(away(p, slot)),
         )
 
+    def win_got(layer, p):
+        return send(win.at[layer, p, most], win.at[layer, p, most], zs.at[layer], zr.at[layer, p], along_z(1))
+
+    def win_sent(layer):
+        return send(down_part.at[layer, most], down_part.at[layer, most], zs.at[layer], zr.at[layer, 0], along_z(1))
+
     def sum_copy(layer, p, k, j):
-        return send(
-            sums.at[layer, p, k], sums.at[layer, p, k], ms.at[layer, p, j], mr.at[layer, p, k], along_z(nc * j)
-        )
+        return send(sums.at[layer, p, k], sums.at[layer, p, k], ms.at[layer], mr.at[layer, p], along_z(nc * j))
+
+    def sum_got(layer, p):
+        three = sums.at[layer, p, pl.ds(0, owners - 1)]
+        return send(three, three, ms.at[layer], mr.at[layer, p], along_z(nc))
+
+    def sum_sent(layer):
+        six = sums.at[layer, pl.ds(0, 2), pl.ds(0, owners - 1)]
+        return send(six, six, ms.at[layer], mr.at[layer, 0], along_z(nc))
 
     def cur_copy(layer, p, b, slot):
         return send(
             cur.at[layer, b, p],
             cur.at[layer, b, p],
-            bs.at[layer, p, slot],
-            br.at[layer, p, slot],
+            bs.at[layer],
+            br.at[layer, b],
             along_z(-away(p, slot)),
         )
 
+    def cur_got(layer, b):
+        return send(cur.at[layer, b], cur.at[layer, b], bs.at[layer], br.at[layer, b], along_z(1))
+
+    def cur_sent(layer):
+        return send(cur.at[layer, most], cur.at[layer, most], bs.at[layer], br.at[layer, 0], along_z(1))
+
     def squares_copy(src, to):
-        return send(squares_row.at[src], squares_row.at[src], ns.at[to], nr.at[src], {"ra": z, "cb": to})
+        return send(squares_row.at[src], squares_row.at[src], ns.at[0], nr.at[0], {"ra": z, "cb": to})
+
+    def squares_all():
+        return send(squares_row.at[most], squares_row.at[most], ns.at[0], nr.at[0], along_c(1))
 
     def inverse_copy(p, b, slot):
-        return send(
-            inverse_row.at[b, p], inverse_row.at[b, p], vs.at[p, slot], vr.at[p, slot], along_z(-away(p, slot))
-        )
+        return send(inverse_row.at[b, p], inverse_row.at[b, p], vs.at[0], vr.at[b], along_z(-away(p, slot)))
+
+    def inverse_got(b):
+        return send(inverse_row.at[b], inverse_row.at[b], vs.at[0], vr.at[b], along_z(1))
+
+    def inverse_sent():
+        return send(inverse_row.at[most], inverse_row.at[most], vs.at[0], vr.at[0], along_z(1))
 
     def near_first(i):
         return (2 * lax.rem(i, 2) - 1) * ((i + 1) // 2)
@@ -255,11 +291,11 @@
             for b in range(1, nc):
                 part_halo[0, b] = p[b - 1, blk - halo :, :].astype(bf16)
             pl.semaphore_wait(barrier, len(peers))
+            greet(0)
             for k in far_c:
                 to = lax.rem(c + k, nc)
                 part_copy(0, to, c).start()
                 halo_copy(0, to, c).start()
-            greet(0)
         else:
 
             def one_block(i, carry, layer=layer):
@@ -267,8 +303,7 @@
 
                 @pl.when(i > 0)
                 def _():
-                    for p in range(2):
-                        cur_copy(layer - 1, p, b, slot_of(p, b)).wait_recv()
+                    cur_got(layer - 1, b).wait_recv()
 
                 p = partials(cur[layer - 1, b].reshape(blk, width).astype(f32), layer)
                 part[layer, b] = p.astype(bf16)
@@ -299,10 +334,10 @@
             greet(1)
             for load in small[2:]:
                 load.wait()
-        for k in range(1, nc):
-            src = lax.rem(c + k, nc)
-            part_copy(layer, c, src).wait_recv()
-            halo_copy(layer, c, src).wait_recv()
+            greeted(1)
+            greet(2)
+        part_all(layer).wait_recv()
+        halo_all(layer).wait_recv()
         for buf, count, at in ((got_halo, halo, 8 - halo), (got, blk, 8)):
             total = buf[layer, 0].astype(f32)
             for src in range(1, nc):
@@ -324,8 +359,8 @@
         for k in far_c:
             hid_copy(layer, c, lax.rem(c + k, nc)).start()
         if layer == 0:
-            greeted(1)
-            greet(2)
+            greeted(2)
+            greet(3)
 
         def down_block(i, carry, layer=layer):
             b = lax.rem(c + near_first(i) + nc, nc)
@@ -350,14 +385,10 @@
         if layer + 1 < layers:
             take_in(layer + 1)
             take_down(layer + 1)
-        if layer == 0:
-            greeted(2)
-            greet(3)
 
         for p in range(2):
             win[layer, p, half - 1 + p] = down_part[layer, mine, p]
-            for slot in others(p):
-                win_copy(layer, p, mine, slot).wait_recv()
+            win_got(layer, p).wait_recv()
             total = win[layer, p, 0].astype(f32)
             for slot in range(1, nc):
                 total = total + win[layer, p, slot].astype(f32)
@@ -368,8 +399,7 @@
                 sum_copy(layer, p, rank, j).start()
         lengths = []
         for p in range(2):
-            for j in far_owner:
-                sum_copy(layer, p, lax.rem(rank + j, owners), j).wait_recv()
+            sum_got(layer, p).wait_recv()
             total = sums[layer, p, 0].astype(f32)
             for k in range(1, owners):
                 total = total + sums[layer, p, k].astype(f32)
@@ -388,8 +418,7 @@
     squares_row[c] = as_row(jnp.concatenate(lengths, axis=0))
     for k in far_c:
         squares_copy(c, lax.rem(c + k, nc)).start()
-    for k in range(1, nc):
-        squares_copy(lax.rem(c + k, nc), c).wait_recv()
+    squares_all().wait_recv()
     total = squares_row[0]
     for k in range(1, nc):
         total = total + squares_row[k]
@@ -402,40 +431,33 @@
 
     last = layers - 1
 
+    def out_copy(b, p):
+        there = pl.ds(pl.multiple_of(b * blk + p * rows, rows), rows)
+        return pltpu.make_async_copy(result.at[b, p], out.at[there], out_sem.at[0])
+
     def put_block(i, carry):
         b = lax.rem(z + near_first(i) + nz, nc)
 
         @pl.when(i > 0)
         def _():
-            for p in range(2):
-                cur_copy(last, p, b, slot_of(p, b)).wait_recv()
-                inverse_copy(p, b, slot_of(p, b)).wait_recv()
+            cur_got(last, b).wait_recv()
+            inverse_got(b).wait_recv()
 
         for p in range(2):
             scale = as_column(inverse_row[b, p], rows, p * rows)
             wide = cur[last, b, p].astype(f32) * scale * gains[layers : layers + 1, :]
-            out[pl.ds(pl.multiple_of(b * blk + p * rows, rows), rows), :] = wide.astype(bf16)
+            result[b, p] = wide.astype(bf16)
+            out_copy(b, p).start()
         return carry
 
     lax.fori_loop(0, nc, put_block, 0)
 
     for layer in range(layers):
-        for k in range(1, nc):
-            to = lax.rem(c + k, nc)
-            part_copy(layer, to, c).wait_send()
-            halo_copy(layer, to, c).wait_send()
-            hid_copy(layer, c, to).wait_send()
-        for p in range(2):
-            for slot in others(p):
-                win_copy(layer, p, lax.rem(z + away(p, slot) + nz, nc), slot).wait_send()
-                cur_copy(layer, p, mine, slot).wait_send()
-            for j in range(1, owners):
-                sum_copy(layer, p, rank, j).wait_send()
-    for k in range(1, nc):
-        squares_copy(c, lax.rem(c + k, nc)).wait_send()
-    for p in range(2):
-        for slot in others(p):
-            inverse_copy(p, mine, slot).wait_send()
+        for sent in (part_all, halo_all, hid_all, win_sent, sum_sent, cur_sent):
+            sent(layer).wait_send()
+    squares_all().wait_send()
+    inverse_sent().wait_send()
+    pltpu.make_async_copy(out, out, out_sem.at[0]).wait()
 
 
 def on_device(
@@ -476,7 +498,7 @@
         functools.partial(kernel, dims),
         out_shape=jax.ShapeDtypeStruct((rows, width), bf16),
         in_specs=[pl.BlockSpec(memory_space=pltpu.HBM)] * len(operands),
-        out_specs=pl.BlockSpec(memory_space=pltpu.VMEM),
+        out_specs=pl.BlockSpec(memory_space=pltpu.HBM),
         scratch_shapes=[pltpu.VMEM(a.shape, a.dtype) for a in small]
         + [
             pltpu.VMEM((layers, 2, ffp, width), f32),
@@ -496,15 +518,16 @@
             pltpu.VMEM((layers, nc, 2, blk // 2, width), bf16),
             pltpu.VMEM((nc, 1, 128), f32),
             pltpu.VMEM((nc, 2, 1, 128), f32),
+            pltpu.VMEM((nc, 2, blk // 2, width), bf16),
             dma((len(small),)),
             dma((layers, 3)),
         ]
-        + [dma((layers, nc))] * 6
-        + [dma((layers, 2, nc))] * 2
-        + [dma((layers, 2, owners))] * 2
-        + [dma((layers, 2, nc))] * 2
-        + [dma((nc,))] * 2
-        + [dma((2, nc))] * 2
+        + [dma((layers,))] * 5
+        + [dma((layers, nc))]
+        + [dma((layers,)), dma((layers, 2))] * 2
+        + [dma((layers,)), dma((layers, nc))]
+        + [dma((1,))] * 3
+        + [dma((nc,)), dma((1,))]
         + [pltpu.SemaphoreType.REGULAR((4,))],
         compiler_params=pltpu.CompilerParams(
             collective_id=0, has_side_effects=True, vmem_limit_bytes=61 * 2**20

time: 143 us -> 145 us (1.014)
  Pallas kernels: 141 us -> 143 us
    pallas_call x1, Pallas kernels: 141 us -> 143 us  [on_device(): pl.pallas_call(functools.partial(kernel, dims), out_shape=jax.ShapeDtypeS...]
where the time goes in v3:
time: 145 us
  Pallas kernels  143 us (99%)
  local copies, waits for them, and re-layouts  1.67 us (1%)
    pallas_call x1, Pallas kernels, on_device(): pl.pallas_call(functools.partial(kernel, dims), out_shape=jax.ShapeDtypeS...  143 us

profile of v3, /device:TPU:40, one launch (start us, length us, event | category | flops | bytes accessed | tf_op | source)
XLA Modules:
  0.0 145.2 jit_solution(10462027542971660374)
XLA Ops:
  0.0 143.5 %shard_map.100 = bf16[256,512]{1,0:T(8,128)(2,1)} custom-call(bf16[256,512]{1,0:T(8,128)(2,1)} %tok_hbm.1, f32[3,512]{1,0:T(4,128)} %gains_hbm.1, f32[2,352,512]{2,1,0:T(8,128)} %bitcast.4, f32[2,352,512]{2,1,0:T(8,128)} %bitcast.5, f32[2,352]{1,0:T(2,128)} %gate_scale_hbm.1, f32[2,352]{1,0:T(2,128)} %value_scale_hbm.1, f32[3,2,352]{2,1,0:T(2,128)} %bitcast.6, ...), custom_call_target="tpu_custom_call" | custom-call | flops 400000000 | bytes 10000000 | tf_op jit(solution)/shard_map/pallas_call | solution.py:497
  143.5 1.7 %copy.12 = bf16[256,512]{1,0:T(8,128)(2,1)} copy(bf16[256,512]{1,0:T(8,128)(2,1)} %shard_map.100) | data formatting | bytes 524288

commit v4 on v3

v4 whole, which is shorter than its diff:
```python
import functools

import jax
import jax.numpy as jnp
from jax import lax
from jax.experimental import pallas as pl
from jax.experimental.pallas import tpu as pltpu
from jax.sharding import PartitionSpec as P

epsilon = 1e-06
residual_weight = 0.5
MESH = pl.DeviceIdType.MESH
f32 = jnp.float32
bf16 = jnp.bfloat16


def in_three(column):
    hi = column.astype(bf16).astype(f32)
    mid = (column - hi).astype(bf16).astype(f32)
    lo = (column - hi - mid).astype(bf16).astype(f32)
    return hi, mid, lo


def with_lanes(tile, at, columns):
    lane = lax.broadcasted_iota(jnp.int32, tile.shape, 1)
    for k, column in enumerate(columns):
        tile = jnp.where(lane == at + k, column, tile)
    return tile


def as_row(column):
    n = column.shape[0]
    at = lax.broadcasted_iota(jnp.int32, (n, 128), 0) == lax.broadcasted_iota(jnp.int32, (n, 128), 1)
    return jnp.sum(jnp.where(at, column, 0.0), axis=0, keepdims=True)


def as_column(row, n):
    at = lax.broadcasted_iota(jnp.int32, (n, 128), 0) == lax.broadcasted_iota(jnp.int32, (n, 128), 1)
    return jnp.sum(jnp.where(at, row, 0.0), axis=1, keepdims=True)


def kernel(
    dims,
    tok_hbm,
    gains_hbm,
    gate_w,
    value_w,
    gate_scale_hbm,
    value_scale_hbm,
    conv_gate_hbm,
    conv_value_hbm,
    down_w,
    down_scale_hbm,
    out,
    tok,
    gains,
    gate_scale,
    value_scale,
    conv_gate,
    conv_value,
    down_scale,
    raw_in,
    raw_down,
    w_first,
    w_later,
    w_down,
    part,
    part_halo,
    got,
    got_halo,
    pre,
    hid,
    down_part,
    win,
    sums,
    cur,
    squares_row,
    inverse_row,
    result,
    small_sem,
    w_sem,
    ps,
    pr,
    qs,
    qr,
    gs,
    gr,
    zs,
    zr,
    ms,
    mr,
    bs,
    br,
    ns,
    nr,
    vs,
    vr,
    out_sem,
    greeting,
):
    layers, nz, nc, width, ff, ffp, blk, taps = dims
    owners = nz // nc
    half = nc // 2
    rows = blk
    halo = taps - 1
    model_width = width * nc
    z = lax.axis_index("ra")
    c = lax.axis_index("cb")
    mine = lax.rem(z, nc)
    rank = z // nc

    def along_z(d):
        return {"ra": lax.rem(z + d + 2 * nz, nz), "cb": c}

    def along_c(k):
        return {"ra": z, "cb": lax.rem(c + k, nc)}

    def send(src, dst, ssem, rsem, to):
        return pltpu.make_async_remote_copy(
            src_ref=src, dst_ref=dst, send_sem=ssem, recv_sem=rsem, device_id=to, device_id_type=MESH
        )

    barrier = pltpu.get_barrier_semaphore()
    peers = [along_c(k) for k in range(1, nc)] + [along_z(1), along_z(-1)]
    for to in peers:
        pl.semaphore_signal(barrier, inc=1, device_id=to, device_id_type=MESH)

    def greet(stage):
        for d in (-(2**stage), 2**stage):
            pl.semaphore_signal(greeting.at[stage], inc=1, device_id=along_z(d), device_id_type=MESH)

    def greeted(stage):
        pl.semaphore_wait(greeting.at[stage], 2)

    def weight_loads(layer):
        for k, (src, dst) in enumerate(
            (
                (gate_w, raw_in.at[layer, 0, pl.ds(0, ff)]),
                (value_w, raw_in.at[layer, 1, pl.ds(0, ff)]),
                (down_w, raw_down.at[layer]),
            )
        ):
            yield pltpu.make_async_copy(src.at[layer], dst, w_sem.at[layer, k])

    small = [
        pltpu.make_async_copy(src, dst, small_sem.at[k])
        for k, (src, dst) in enumerate(
            (
                (tok_hbm, tok),
                (gains_hbm, gains),
                (gate_scale_hbm, gate_scale),
                (value_scale_hbm, value_scale),
                (conv_gate_hbm, conv_gate),
                (conv_value_hbm, conv_value),
                (down_scale_hbm, down_scale),
            )
        )
    ]
    weights = [list(weight_loads(layer)) for layer in range(layers)]
    for load in small[:2] + weights[0] + small[2:] + sum(weights[1:], []):
        load.start()

    edge = ff // 128 * 128
    for layer in range(layers):
        for s in range(2):
            raw_in[layer, s, ff:, :] = jnp.zeros((ffp - ff, width), f32)
        w_down[layer, ff:, :] = jnp.zeros((ffp - ff, width), bf16)
        part_halo[layer, 0, 0] = jnp.zeros((halo, 2 * ffp), bf16)
        for p in range(2):
            hid[layer, p, c, :, edge:] = jnp.zeros((blk, ffp - edge), bf16)

    def take_in(layer):
        for s in range(2):
            weights[layer][s].wait()
            if layer == 0:
                w_first[s * ffp : (s + 1) * ffp, :] = raw_in[0, s].astype(bf16)
            else:
                w_later[layer - 1, :, s * ffp : (s + 1) * ffp] = raw_in[layer, s].T.astype(bf16)

    def take_down(layer):
        weights[layer][2].wait()
        w_down[layer, 0:ff, :] = raw_down[layer].astype(bf16)

    def partials(x, layer):
        scaled = (x * gains[layer : layer + 1, :]).astype(bf16)
        if layer == 0:
            p = lax.dot_general(scaled, w_first[...], (((1,), (1,)), ((), ())), preferred_element_type=f32)
        else:
            p = jnp.dot(scaled, w_later[layer - 1], preferred_element_type=f32)
        squares = in_three(jnp.sum(x * x, axis=1, keepdims=True))
        last = with_lanes(p[:, edge:ffp], ff - edge, squares)
        return jnp.concatenate([p[:, :edge], last, p[:, ffp:]], axis=1)

    most = pl.ds(0, nc - 1)

    def part_copy(layer, p, b):
        return send(part.at[layer, p, b], got.at[layer, p, c], ps.at[layer], pr.at[layer, p], {"ra": z, "cb": b})

    def part_got(layer, p):
        ref = got.at[layer, p, most]
        return send(ref, ref, ps.at[layer], pr.at[layer, p], along_c(1))

    def part_sent(layer):
        ref = part.at[layer, pl.ds(0, 2), most]
        return send(ref, ref, ps.at[layer], pr.at[layer, 0], along_c(1))

    def halo_copy(layer, p, b):
        return send(
            part_halo.at[layer, p, b], got_halo.at[layer, p, c], qs.at[layer], qr.at[layer, p], {"ra": z, "cb": b}
        )

    def halo_got(layer, p):
        ref = got_halo.at[layer, p, most]
        return send(ref, ref, qs.at[layer], qr.at[layer, p], along_c(1))

    def halo_sent(layer):
        ref = part_halo.at[layer, pl.ds(0, 2), most]
        return send(ref, ref, qs.at[layer], qr.at[layer, 0], along_c(1))

    def hid_copy(layer, p, b, to):
        return send(hid.at[layer, p, b], hid.at[layer, p, b], gs.at[layer], gr.at[layer, p, b], {"ra": z, "cb": to})

    def hid_sent(layer):
        ref = hid.at[layer, pl.ds(0, 2), most]
        return send(ref, ref, gs.at[layer], gr.at[layer, 0, 0], along_c(1))

    def away(p, slot):
        return slot - (half - 1) - p

    def slot_of(p, b):
        return lax.rem(b - z + (half - 1) + p + nz, nc)

    def others(p):
        return sorted((s for s in range(nc) if away(p, s) != 0), key=lambda s: -abs(away(p, s)))

    def win_copy(layer, p, b, slot):
        return send(
            down_part.at[layer, p, b],
            win.at[layer, p, slot],
            zs.at[layer],
            zr.at[layer, p],
            along_z(away(p, slot)),
        )

    def win_got(layer, p):
        return send(win.at[layer, p, most], win.at[layer, p, most], zs.at[layer], zr.at[layer, p], along_z(1))

    def win_sent(layer):
        ref = down_part.at[layer, pl.ds(0, 2), most]
        return send(ref, ref, zs.at[layer], zr.at[layer, 0], along_z(1))

    def sum_copy(layer, p, k, j):
        return send(sums.at[layer, p, k], sums.at[layer, p, k], ms.at[layer], mr.at[layer, p], along_z(nc * j))

    def sum_got(layer, p):
        three = sums.at[layer, p, pl.ds(0, owners - 1)]
        return send(three, three, ms.at[layer], mr.at[layer, p], along_z(nc))

    def sum_sent(layer):
        six = sums.at[layer, pl.ds(0, 2), pl.ds(0, owners - 1)]
        return send(six, six, ms.at[layer], mr.at[layer, 0], along_z(nc))

    def cur_copy(layer, p, b, slot):
        ref = cur.at[layer, p, b]
        return send(ref, ref, bs.at[layer], br.at[layer, p, b], along_z(-away(p, slot)))

    def cur_got(layer, p, b):
        ref = cur.at[layer, p, b]
        return send(ref, ref, bs.at[layer], br.at[layer, p, b], along_z(1))

    def cur_sent(layer):
        ref = cur.at[layer, pl.ds(0, 2), most]
        return send(ref, ref, bs.at[layer], br.at[layer, 0, 0], along_z(1))

    def squares_copy(p, to):
        ref = squares_row.at[p, c]
        return send(ref, ref, ns.at[0], nr.at[p], {"ra": z, "cb": to})

    def squares_got(p):
        ref = squares_row.at[p, most]
        return send(ref, ref, ns.at[0], nr.at[p], along_c(1))

    def squares_sent():
        ref = squares_row.at[pl.ds(0, 2), most]
        return send(ref, ref, ns.at[0], nr.at[0], along_c(1))

    def inverse_copy(p, b, slot):
        ref = inverse_row.at[p, b]
        return send(ref, ref, vs.at[0], vr.at[p, b], along_z(-away(p, slot)))

    def inverse_got(p, b):
        ref = inverse_row.at[p, b]
        return send(ref, ref, vs.at[0], vr.at[p, b], along_z(1))

    def inverse_sent():
        ref = inverse_row.at[pl.ds(0, 2), most]
        return send(ref, ref, vs.at[0], vr.at[0, 0], along_z(1))

    def near_first(i):
        return (2 * lax.rem(i, 2) - 1) * ((i + 1) // 2)

    far_c = sorted(range(1, nc), key=lambda k: -min(k, nc - k))
    far_owner = sorted(range(1, owners), key=lambda j: -min(j, owners - j))

    for layer in range(layers):
        if layer == 0:
            small[0].wait()
            small[1].wait()
            take_in(0)
            y = partials(tok[...].astype(f32), 0).reshape(2, nc, blk, 2 * ffp)
            part[0] = y.astype(bf16)
            for p in range(2):
                for b in range(nc):
                    if p + b > 0:
                        before = (p, b - 1) if b > 0 else (p - 1, nc - 1)
                        part_halo[0, p, b] = y[before][blk - halo :, :].astype(bf16)
            pl.semaphore_wait(barrier, len(peers))
            greet(0)
            for p in range(2):
                for k in far_c:
                    to = lax.rem(c + k, nc)
                    part_copy(0, p, to).start()
                    halo_copy(0, p, to).start()
        else:
            for p in range(2):
                if p == 0:

                    @pl.when(c != 0)
                    def _(layer=layer):
                        halo_copy(layer, 0, 0).start()

                def two_blocks(i, carry, layer=layer, p=p):
                    b0 = lax.rem(z + near_first(2 * i) + nz, nc)
                    b1 = lax.rem(z + near_first(2 * i + 1) + nz, nc)

                    @pl.when(i > 0)
                    def _():
                        cur_got(layer - 1, p, b0).wait_recv()

                    cur_got(layer - 1, p, b1).wait_recv()
                    x = jnp.concatenate([cur[layer - 1, p, b0], cur[layer - 1, p, b1]], axis=0)
                    y = partials(x.astype(f32), layer)
                    for b, first in ((b0, 0), (b1, blk)):
                        part[layer, p, b] = y[first : first + blk, :].astype(bf16)

                        @pl.when(b != c)
                        def _(b=b):
                            part_copy(layer, p, b).start()

                        ends = y[first + blk - halo : first + blk, :].astype(bf16)
                        after = lax.rem(b + 1, nc)

                        @pl.when(after != 0)
                        def _(after=after, ends=ends):
                            part_halo[layer, p, after] = ends

                            @pl.when(after != c)
                            def _():
                                halo_copy(layer, p, after).start()

                        if p == 0:

                            @pl.when(after == 0)
                            def _(ends=ends):
                                part_halo[layer, 1, 0] = ends

                                @pl.when(c != 0)
                                def _():
                                    halo_copy(layer, 1, 0).start()

                    return carry

                lax.fori_loop(0, nc // 2, two_blocks, 0)

        if layer == 0:
            take_down(0)
            greeted(0)
            greet(1)
            for load in small[2:]:
                load.wait()
            greeted(1)
            greet(2)
        for p in range(2):
            got[layer, p, c] = part[layer, p, c]
            got_halo[layer, p, c] = part_halo[layer, p, c]
            part_got(layer, p).wait_recv()
            halo_got(layer, p).wait_recv()
            for buf, count, at in ((got_halo, halo, 8 - halo), (got, blk, 8)):
                total = buf[layer, p, 0].astype(f32)
                for src in range(1, nc):
                    total = total + buf[layer, p, src].astype(f32)
                squares = jnp.sum(total[:, ff : ff + 3], axis=1, keepdims=True)
                inverse = lax.rsqrt(squares / model_width + epsilon)
                pre[p, at : at + count, 0:ff] = inverse * gate_scale[layer : layer + 1, :] * total[:, 0:ff]
                pre[p, at : at + count, ffp : ffp + ff] = (
                    inverse * value_scale[layer : layer + 1, :] * total[:, ffp : ffp + ff]
                )
            convs = []
            for lane, tap_weights in ((0, conv_gate), (ffp, conv_value)):
                y = None
                for k in range(taps):
                    at = 8 - halo + k
                    term = pre[p, at : at + blk, lane : lane + ff] * tap_weights[k, layer : layer + 1, :]
                    y = term if y is None else y + term
                convs.append(y)
            hid[layer, p, c, :, 0:ff] = (jax.nn.gelu(convs[0], approximate=True) * convs[1]).astype(bf16)
            for k in far_c:
                hid_copy(layer, p, c, lax.rem(c + k, nc)).start()
        if layer == 0:
            greeted(2)
            greet(3)

        for p in range(2):

            def two_downs(i, carry, layer=layer, p=p):
                b0 = lax.rem(c + near_first(2 * i) + nc, nc)
                b1 = lax.rem(c + near_first(2 * i + 1) + nc, nc)

                @pl.when(i > 0)
                def _():
                    hid_copy(layer, p, b0, c).wait_recv()

                hid_copy(layer, p, b1, c).wait_recv()
                h = jnp.concatenate([hid[layer, p, b0], hid[layer, p, b1]], axis=0)
                d = jnp.dot(h, w_down[layer], preferred_element_type=f32).astype(bf16)
                for b, first in ((b0, 0), (b1, blk)):
                    down_part[layer, p, b] = d[first : first + blk, :]
                    slot = slot_of(p, b)

                    @pl.when(slot != half - 1 + p)
                    def _(b=b, slot=slot):
                        win_copy(layer, p, b, slot).start()

                return carry

            lax.fori_loop(0, nc // 2, two_downs, 0)
        if layer + 1 < layers:
            take_in(layer + 1)
            take_down(layer + 1)

        for p in range(2):
            win[layer, p, half - 1 + p] = down_part[layer, p, mine]
            win_got(layer, p).wait_recv()
            total = win[layer, p, 0].astype(f32)
            for slot in range(1, nc):
                total = total + win[layer, p, slot].astype(f32)
            sums[layer, p, rank] = total.astype(bf16)
            if layer == 0 and p == 0:
                greeted(3)
            for j in far_owner:
                sum_copy(layer, p, rank, j).start()
        for p in range(2):
            sum_got(layer, p).wait_recv()
            total = sums[layer, p, 0].astype(f32)
            for k in range(1, owners):
                total = total + sums[layer, p, k].astype(f32)
            if layer == 0:
                own = tok[pl.ds(pl.multiple_of((p * nc + mine) * blk, blk), blk), :].astype(f32)
            else:
                own = cur[layer - 1, p, mine].astype(f32)
            new = (residual_weight * own + down_scale[layer : layer + 1, :] * total).astype(bf16)
            cur[layer, p, mine] = new
            for slot in others(p):
                cur_copy(layer, p, mine, slot).start()
            if layer == layers - 1:
                wide = new.astype(f32)
                squares_row[p, c] = as_row(jnp.sum(wide * wide, axis=1, keepdims=True))
                for k in far_c:
                    squares_copy(p, lax.rem(c + k, nc)).start()

    for p in range(2):
        squares_got(p).wait_recv()
        total = squares_row[p, 0]
        for k in range(1, nc):
            total = total + squares_row[p, k]
        inverse_row[p, mine] = lax.rsqrt(total / model_width + epsilon)
        for slot in others(p):
            inverse_copy(p, mine, slot).start()

    last = layers - 1

    def out_copy(p, b):
        there = pl.ds(pl.multiple_of((p * nc + b) * blk, blk), blk)
        return pltpu.make_async_copy(result.at[p, b], out.at[there], out_sem.at[0])

    for p in range(2):

        def put_block(i, carry, p=p):
            b = lax.rem(z + near_first(i) + nz, nc)

            @pl.when(i > 0)
            def _():
                cur_got(last, p, b).wait_recv()
                inverse_got(p, b).wait_recv()

            scale = as_column(inverse_row[p, b], blk)
            wide = cur[last, p, b].astype(f32) * scale * gains[layers : layers + 1, :]
            result[p, b] = wide.astype(bf16)
            out_copy(p, b).start()
            return carry

        lax.fori_loop(0, nc, put_block, 0)

    for layer in range(layers):
        for sent in (part_sent, halo_sent, hid_sent, win_sent, sum_sent, cur_sent):
            sent(layer).wait_send()
    squares_sent().wait_send()
    inverse_sent().wait_send()
    pltpu.make_async_copy(out, out, out_sem.at[0]).wait()


def on_device(
    tokens,
    norm_gains,
    gate_weight,
    value_weight,
    gate_scale,
    value_scale,
    conv_gate,
    conv_value,
    down_weight,
    down_scale,
):
    nz, nc = lax.axis_size("ra"), lax.axis_size("cb")
    rows, width = tokens.shape
    layers, _, ff = gate_weight.shape
    taps = conv_gate.shape[1]
    ffp = (ff + 3 + 127) // 128 * 128
    blk = rows // (2 * nc)
    owners = nz // nc
    dims = (layers, nz, nc, width, ff, ffp, blk, taps)
    dma = pltpu.SemaphoreType.DMA
    operands = (
        tokens,
        norm_gains,
        gate_weight.swapaxes(1, 2),
        value_weight.swapaxes(1, 2),
        gate_scale,
        value_scale,
        conv_gate.swapaxes(0, 1),
        conv_value.swapaxes(0, 1),
        down_weight,
        down_scale,
    )
    small = [operands[k] for k in (0, 1, 4, 5, 6, 7, 9)]
    return pl.pallas_call(
        functools.partial(kernel, dims),
        out_shape=jax.ShapeDtypeStruct((rows, width), bf16),
        in_specs=[pl.BlockSpec(memory_space=pltpu.HBM)] * len(operands),
        out_specs=pl.BlockSpec(memory_space=pltpu.HBM),
        scratch_shapes=[pltpu.VMEM(a.shape, a.dtype) for a in small]
        + [
            pltpu.VMEM((layers, 2, ffp, width), f32),
            pltpu.VMEM((layers, ff, width), f32),
            pltpu.VMEM((2 * ffp, width), bf16),
            pltpu.VMEM((layers - 1, width, 2 * ffp), bf16),
            pltpu.VMEM((layers, ffp, width), bf16),
            pltpu.VMEM((layers, 2, nc, blk, 2 * ffp), bf16),
            pltpu.VMEM((layers, 2, nc, taps - 1, 2 * ffp), bf16),
            pltpu.VMEM((layers, 2, nc, blk, 2 * ffp), bf16),
            pltpu.VMEM((layers, 2, nc, taps - 1, 2 * ffp), bf16),
            pltpu.VMEM((2, 8 + blk, 2 * ffp), f32),
            pltpu.VMEM((layers, 2, nc, blk, ffp), bf16),
            pltpu.VMEM((layers, 2, nc, blk, width), bf16),
            pltpu.VMEM((layers, 2, nc, blk, width), bf16),
            pltpu.VMEM((layers, 2, owners, blk, width), bf16),
            pltpu.VMEM((layers, 2, nc, blk, width), bf16),
            pltpu.VMEM((2, nc, 1, 128), f32),
            pltpu.VMEM((2, nc, 1, 128), f32),
            pltpu.VMEM((2, nc, blk, width), bf16),
            dma((len(small),)),
            dma((layers, 3)),
        ]
        + [dma((layers,)), dma((layers, 2))] * 2
        + [dma((layers,)), dma((layers, 2, nc))]
        + [dma((layers,)), dma((layers, 2))] * 2
        + [dma((layers,)), dma((layers, 2, nc))]
        + [dma((1,)), dma((2,)), dma((1,)), dma((2, nc)), dma((1,))]
        + [pltpu.SemaphoreType.REGULAR((4,))],
        compiler_params=pltpu.CompilerParams(
            collective_id=0, has_side_effects=True, vmem_limit_bytes=61 * 2**20
        ),
        cost_estimate=pl.CostEstimate(flops=4 * 10**8, bytes_accessed=10**7, transcendentals=0),
    )(*operands)


def solution(mesh):
    in_specs = (
        P("grp", "cb"),
        P(None, "cb"),
        P(None, "cb", "ra"),
        P(None, "cb", "ra"),
        P(None, "ra"),
        P(None, "ra"),
        P(None, None, "ra"),
        P(None, None, "ra"),
        P(None, "ra", "cb"),
        P(None, "cb"),
    )
    out_specs = P("grp", "cb")
    return jax.shard_map(on_device, mesh=mesh, in_specs=in_specs, out_specs=out_specs, check_vma=False)
```

time: 145 us -> 141 us (0.972)
  Pallas kernels: 143 us -> 139 us
    pallas_call x1, Pallas kernels: 143 us -> 139 us  [on_device(): pl.pallas_call(functools.partial(kernel, dims), out_shape=jax.ShapeDtypeS...]
where the time goes in v4:
time: 141 us
  Pallas kernels  139 us (99%)
  local copies, waits for them, and re-layouts  1.67 us (1%)
    pallas_call x1, Pallas kernels, on_device(): pl.pallas_call(functools.partial(kernel, dims), out_shape=jax.ShapeDtypeS...  139 us

profile of v4, /device:TPU:40, one launch (start us, length us, event | category | flops | bytes accessed | tf_op | source)
XLA Modules:
  0.0 140.7 jit_solution(5734152457767651299)
XLA Ops:
  0.0 139.0 %shard_map.100 = bf16[256,512]{1,0:T(8,128)(2,1)} custom-call(bf16[256,512]{1,0:T(8,128)(2,1)} %tok_hbm.1, f32[3,512]{1,0:T(4,128)} %gains_hbm.1, f32[2,352,512]{2,1,0:T(8,128)} %bitcast.4, f32[2,352,512]{2,1,0:T(8,128)} %bitcast.5, f32[2,352]{1,0:T(2,128)} %gate_scale_hbm.1, f32[2,352]{1,0:T(2,128)} %value_scale_hbm.1, f32[3,2,352]{2,1,0:T(2,128)} %bitcast.6, ...), custom_call_target="tpu_custom_call" | custom-call | flops 400000000 | bytes 10000000 | tf_op jit(solution)/shard_map/pallas_call | solution.py:546
  139.0 1.7 %copy.12 = bf16[256,512]{1,0:T(8,128)(2,1)} copy(bf16[256,512]{1,0:T(8,128)(2,1)} %shard_map.100) | data formatting | bytes 524288

commit v5 on v4

--- a/solution.py
+++ b/solution.py
@@ -249,16 +249,26 @@
         ref = down_part.at[layer, pl.ds(0, 2), most]
         return send(ref, ref, zs.at[layer], zr.at[layer, 0], along_z(1))
 
-    def sum_copy(layer, p, k, j):
-        return send(sums.at[layer, p, k], sums.at[layer, p, k], ms.at[layer], mr.at[layer, p], along_z(nc * j))
-
-    def sum_got(layer, p):
-        three = sums.at[layer, p, pl.ds(0, owners - 1)]
-        return send(three, three, ms.at[layer], mr.at[layer, p], along_z(nc))
+    upward = nc * (1 - 2 * lax.rem(rank, 2))
+
+    def sum_copies(layer, p, turn):
+        for h, sign in enumerate((1, -1) if turn == 0 else (-1, 1)):
+            columns = pl.ds(h * (width // 2), width // 2)
+            yield send(
+                sums.at[layer, p, 2 * turn, :, columns],
+                sums.at[layer, p, 2 * turn + 1, :, columns],
+                ms.at[layer],
+                mr.at[layer, p, turn],
+                along_z(sign * upward),
+            )
+
+    def sum_got(layer, p, turn):
+        ref = sums.at[layer, p, 2 * turn + 1]
+        return send(ref, ref, ms.at[layer], mr.at[layer, p, turn], along_z(nc))
 
     def sum_sent(layer):
-        six = sums.at[layer, pl.ds(0, 2), pl.ds(0, owners - 1)]
-        return send(six, six, ms.at[layer], mr.at[layer, 0], along_z(nc))
+        ref = sums.at[layer, pl.ds(0, 2), pl.ds(0, 2)]
+        return send(ref, ref, ms.at[layer], mr.at[layer, 0, 0], along_z(nc))
 
     def cur_copy(layer, p, b, slot):
         ref = cur.at[layer, p, b]
@@ -300,7 +310,21 @@
         return (2 * lax.rem(i, 2) - 1) * ((i + 1) // 2)
 
     far_c = sorted(range(1, nc), key=lambda k: -min(k, nc - k))
-    far_owner = sorted(range(1, owners), key=lambda j: -min(j, owners - j))
+
+    def finish(layer, p, total):
+        if layer == 0:
+            own = tok[pl.ds(pl.multiple_of((p * nc + mine) * blk, blk), blk), :].astype(f32)
+        else:
+            own = cur[layer - 1, p, mine].astype(f32)
+        new = (residual_weight * own + down_scale[layer : layer + 1, :] * total).astype(bf16)
+        cur[layer, p, mine] = new
+        for slot in others(p):
+            cur_copy(layer, p, mine, slot).start()
+        if layer == layers - 1:
+            wide = new.astype(f32)
+            squares_row[p, c] = as_row(jnp.sum(wide * wide, axis=1, keepdims=True))
+            for k in far_c:
+                squares_copy(p, lax.rem(c + k, nc)).start()
 
     for layer in range(layers):
         if layer == 0:
@@ -406,9 +430,6 @@
             hid[layer, p, c, :, 0:ff] = (jax.nn.gelu(convs[0], approximate=True) * convs[1]).astype(bf16)
             for k in far_c:
                 hid_copy(layer, p, c, lax.rem(c + k, nc)).start()
-        if layer == 0:
-            greeted(2)
-            greet(3)
 
         for p in range(2):
 
@@ -444,29 +465,21 @@
             total = win[layer, p, 0].astype(f32)
             for slot in range(1, nc):
                 total = total + win[layer, p, slot].astype(f32)
-            sums[layer, p, rank] = total.astype(bf16)
+            sums[layer, p, 0] = total.astype(bf16)
             if layer == 0 and p == 0:
-                greeted(3)
-            for j in far_owner:
-                sum_copy(layer, p, rank, j).start()
-        for p in range(2):
-            sum_got(layer, p).wait_recv()
-            total = sums[layer, p, 0].astype(f32)
-            for k in range(1, owners):
-                total = total + sums[layer, p, k].astype(f32)
-            if layer == 0:
-                own = tok[pl.ds(pl.multiple_of((p * nc + mine) * blk, blk), blk), :].astype(f32)
-            else:
-                own = cur[layer - 1, p, mine].astype(f32)
-            new = (residual_weight * own + down_scale[layer : layer + 1, :] * total).astype(bf16)
-            cur[layer, p, mine] = new
-            for slot in others(p):
-                cur_copy(layer, p, mine, slot).start()
-            if layer == layers - 1:
-                wide = new.astype(f32)
-                squares_row[p, c] = as_row(jnp.sum(wide * wide, axis=1, keepdims=True))
-                for k in far_c:
-                    squares_copy(p, lax.rem(c + k, nc)).start()
+                greeted(2)
+            for copy in sum_copies(layer, p, 0):
+                copy.start()
+        for turn in range(2):
+            for p in range(2):
+                sum_got(layer, p, turn).wait_recv()
+                both = sums[layer, p, 2 * turn].astype(f32) + sums[layer, p, 2 * turn + 1].astype(f32)
+                if turn == 0:
+                    sums[layer, p, 2] = both.astype(bf16)
+                    for copy in sum_copies(layer, p, 1):
+                        copy.start()
+                else:
+                    finish(layer, p, both)
 
     for p in range(2):
         squares_got(p).wait_recv()
@@ -573,10 +586,10 @@
         ]
         + [dma((layers,)), dma((layers, 2))] * 2
         + [dma((layers,)), dma((layers, 2, nc))]
-        + [dma((layers,)), dma((layers, 2))] * 2
+        + [dma((layers,)), dma((layers, 2)), dma((layers,)), dma((layers, 2, 2))]
         + [dma((layers,)), dma((layers, 2, nc))]
         + [dma((1,)), dma((2,)), dma((1,)), dma((2, nc)), dma((1,))]
-        + [pltpu.SemaphoreType.REGULAR((4,))],
+        + [pltpu.SemaphoreType.REGULAR((3,))],
         compiler_params=pltpu.CompilerParams(
             collective_id=0, has_side_effects=True, vmem_limit_bytes=61 * 2**20
         ),

time: 141 us -> 126 us (0.89)
  Pallas kernels: 139 us -> 124 us
    pallas_call x1, Pallas kernels: 139 us -> 124 us  [on_device(): pl.pallas_call(functools.partial(kernel, dims), out_shape=jax.ShapeDtypeS...]
where the time goes in v5:
time: 126 us
  Pallas kernels  124 us (98%)
  local copies, waits for them, and re-layouts  1.67 us (1%)
    pallas_call x1, Pallas kernels, on_device(): pl.pallas_call(functools.partial(kernel, dims), out_shape=jax.ShapeDtypeS...  124 us

profile of v5, /device:TPU:40, one launch (start us, length us, event | category | flops | bytes accessed | tf_op | source)
XLA Modules:
  0.0 126.1 jit_solution(1492970914554495399)
XLA Ops:
  0.0 124.4 %shard_map.100 = bf16[256,512]{1,0:T(8,128)(2,1)} custom-call(bf16[256,512]{1,0:T(8,128)(2,1)} %tok_hbm.1, f32[3,512]{1,0:T(4,128)} %gains_hbm.1, f32[2,352,512]{2,1,0:T(8,128)} %bitcast.4, f32[2,352,512]{2,1,0:T(8,128)} %bitcast.5, f32[2,352]{1,0:T(2,128)} %gate_scale_hbm.1, f32[2,352]{1,0:T(2,128)} %value_scale_hbm.1, f32[3,2,352]{2,1,0:T(2,128)} %bitcast.6, ...), custom_call_target="tpu_custom_call" | custom-call | flops 400000000 | bytes 10000000 | tf_op jit(solution)/shard_map/pallas_call | solution.py:559
  124.4 1.7 %copy.12 = bf16[256,512]{1,0:T(8,128)(2,1)} copy(bf16[256,512]{1,0:T(8,128)(2,1)} %shard_map.100) | data formatting | bytes 524288

commit v6 on v5

--- a/solution.py
+++ b/solution.py
@@ -224,23 +224,28 @@
         ref = hid.at[layer, pl.ds(0, 2), most]
         return send(ref, ref, gs.at[layer], gr.at[layer, 0, 0], along_c(1))
 
-    def away(p, slot):
-        return slot - (half - 1) - p
-
-    def slot_of(p, b):
-        return lax.rem(b - z + (half - 1) + p + nz, nc)
-
-    def others(p):
-        return sorted((s for s in range(nc) if away(p, s) != 0), key=lambda s: -abs(away(p, s)))
+    here, split = half - 1, nc - 1
+    left, right = pl.ds(0, width // 2), pl.ds(width // 2, width // 2)
+
+    def slot_of(b):
+        return lax.rem(b - z + here + nz, nc)
+
+    others = [split] + sorted((s for s in range(nc - 1) if s != here), key=lambda s: -abs(s - here))
 
     def win_copy(layer, p, b, slot):
         return send(
-            down_part.at[layer, p, b],
-            win.at[layer, p, slot],
-            zs.at[layer],
-            zr.at[layer, p],
-            along_z(away(p, slot)),
+            down_part.at[layer, p, b], win.at[layer, p, slot], zs.at[layer], zr.at[layer, p], along_z(slot - here)
         )
+
+    def win_halves(layer, p, b):
+        for columns, d in ((left, half), (right, -half)):
+            yield send(
+                down_part.at[layer, p, b, :, columns],
+                win.at[layer, p, split, :, columns],
+                zs.at[layer],
+                zr.at[layer, p],
+                along_z(d),
+            )
 
     def win_got(layer, p):
         return send(win.at[layer, p, most], win.at[layer, p, most], zs.at[layer], zr.at[layer, p], along_z(1))
@@ -270,9 +275,15 @@
         ref = sums.at[layer, pl.ds(0, 2), pl.ds(0, 2)]
         return send(ref, ref, ms.at[layer], mr.at[layer, 0, 0], along_z(nc))
 
-    def cur_copy(layer, p, b, slot):
-        ref = cur.at[layer, p, b]
-        return send(ref, ref, bs.at[layer], br.at[layer, p, b], along_z(-away(p, slot)))
+    def cur_copies(layer, p, b):
+        for slot in others:
+            if slot == split:
+                for columns, d in ((left, -half), (right, half)):
+                    ref = cur.at[layer, p, b, :, columns]
+                    yield send(ref, ref, bs.at[layer], br.at[layer, p, b], along_z(d))
+            else:
+                ref = cur.at[layer, p, b]
+                yield send(ref, ref, bs.at[layer], br.at[layer, p, b], along_z(here - slot))
 
     def cur_got(layer, p, b):
         ref = cur.at[layer, p, b]
@@ -296,7 +307,7 @@
 
     def inverse_copy(p, b, slot):
         ref = inverse_row.at[p, b]
-        return send(ref, ref, vs.at[0], vr.at[p, b], along_z(-away(p, slot)))
+        return send(ref, ref, vs.at[0], vr.at[p, b], along_z(here - slot))
 
     def inverse_got(p, b):
         ref = inverse_row.at[p, b]
@@ -317,30 +328,33 @@
         else:
             own = cur[layer - 1, p, mine].astype(f32)
         new = (residual_weight * own + down_scale[layer : layer + 1, :] * total).astype(bf16)
-        cur[layer, p, mine] = new
-        for slot in others(p):
-            cur_copy(layer, p, mine, slot).start()
         if layer == layers - 1:
             wide = new.astype(f32)
             squares_row[p, c] = as_row(jnp.sum(wide * wide, axis=1, keepdims=True))
             for k in far_c:
                 squares_copy(p, lax.rem(c + k, nc)).start()
+        cur[layer, p, mine] = new
+        for copy in cur_copies(layer, p, mine):
+            copy.start()
 
     for layer in range(layers):
         if layer == 0:
             small[0].wait()
             small[1].wait()
             take_in(0)
-            y = partials(tok[...].astype(f32), 0).reshape(2, nc, blk, 2 * ffp)
-            part[0] = y.astype(bf16)
+            before = None
             for p in range(2):
-                for b in range(nc):
-                    if p + b > 0:
-                        before = (p, b - 1) if b > 0 else (p - 1, nc - 1)
-                        part_halo[0, p, b] = y[before][blk - halo :, :].astype(bf16)
-            pl.semaphore_wait(barrier, len(peers))
-            greet(0)
-            for p in range(2):
+                y = partials(tok[p * nc * blk : (p + 1) * nc * blk, :].astype(f32), 0).reshape(nc, blk, 2 * ffp)
+                part[0, p] = y.astype(bf16)
+                ends = y[:, blk - halo :, :].astype(bf16)
+                if p > 0:
+                    part_halo[0, p, 0] = before
+                for b in range(1, nc):
+                    part_halo[0, p, b] = ends[b - 1]
+                before = ends[nc - 1]
+                if p == 0:
+                    pl.semaphore_wait(barrier, len(peers))
+                    greet(0)
                 for k in far_c:
                     to = lax.rem(c + k, nc)
                     part_copy(0, p, to).start()
@@ -446,11 +460,16 @@
                 d = jnp.dot(h, w_down[layer], preferred_element_type=f32).astype(bf16)
                 for b, first in ((b0, 0), (b1, blk)):
                     down_part[layer, p, b] = d[first : first + blk, :]
-                    slot = slot_of(p, b)
-
-                    @pl.when(slot != half - 1 + p)
+                    slot = slot_of(b)
+
+                    @pl.when(jnp.logical_and(slot != here, slot != split))
                     def _(b=b, slot=slot):
                         win_copy(layer, p, b, slot).start()
+
+                    @pl.when(slot == split)
+                    def _(b=b):
+                        for copy in win_halves(layer, p, b):
+                            copy.start()
 
                 return carry
 
@@ -460,7 +479,7 @@
             take_down(layer + 1)
 
         for p in range(2):
-            win[layer, p, half - 1 + p] = down_part[layer, p, mine]
+            win[layer, p, here] = down_part[layer, p, mine]
             win_got(layer, p).wait_recv()
             total = win[layer, p, 0].astype(f32)
             for slot in range(1, nc):
@@ -487,7 +506,7 @@
         for k in range(1, nc):
             total = total + squares_row[p, k]
         inverse_row[p, mine] = lax.rsqrt(total / model_width + epsilon)
-        for slot in others(p):
+        for slot in others:
             inverse_copy(p, mine, slot).start()
 
     last = layers - 1

time: 126 us -> 126 us (level)
  no operation moved by 1% of the time
where the time goes in v6:
time: 126 us; the launch traced here: 125 us
  Pallas kernels  124 us (98%)
  local copies, waits for them, and re-layouts  1.67 us (1%)
    pallas_call x1, Pallas kernels, on_device(): pl.pallas_call(functools.partial(kernel, dims), out_shape=jax.ShapeDtypeS...  124 us

profile of v6, /device:TPU:40, one launch (start us, length us, event | category | flops | bytes accessed | tf_op | source)
XLA Modules:
  0.0 125.4 jit_solution(1615512480706103205)
XLA Ops:
  0.0 123.7 %shard_map.100 = bf16[256,512]{1,0:T(8,128)(2,1)} custom-call(bf16[256,512]{1,0:T(8,128)(2,1)} %tok_hbm.1, f32[3,512]{1,0:T(4,128)} %gains_hbm.1, f32[2,352,512]{2,1,0:T(8,128)} %bitcast.4, f32[2,352,512]{2,1,0:T(8,128)} %bitcast.5, f32[2,352]{1,0:T(2,128)} %gate_scale_hbm.1, f32[2,352]{1,0:T(2,128)} %value_scale_hbm.1, f32[3,2,352]{2,1,0:T(2,128)} %bitcast.6, ...), custom_call_target="tpu_custom_call" | custom-call | flops 400000000 | bytes 10000000 | tf_op jit(solution)/shard_map/pallas_call | solution.py:578
  123.7 1.7 %copy.12 = bf16[256,512]{1,0:T(8,128)(2,1)} copy(bf16[256,512]{1,0:T(8,128)(2,1)} %shard_map.100) | data formatting | bytes 524288

commit v7 on v6

--- a/solution.py
+++ b/solution.py
@@ -225,65 +225,55 @@
         return send(ref, ref, gs.at[layer], gr.at[layer, 0, 0], along_c(1))
 
     here, split = half - 1, nc - 1
-    left, right = pl.ds(0, width // 2), pl.ds(width // 2, width // 2)
+    sides = (pl.ds(0, width // 2), pl.ds(width // 2, width // 2))
+    side = (slice(0, width // 2), slice(width // 2, width))
 
     def slot_of(b):
         return lax.rem(b - z + here + nz, nc)
 
     others = [split] + sorted((s for s in range(nc - 1) if s != here), key=lambda s: -abs(s - here))
 
-    def win_copy(layer, p, b, slot):
+    def win_copy(layer, p, h, b, slot, d):
         return send(
-            down_part.at[layer, p, b], win.at[layer, p, slot], zs.at[layer], zr.at[layer, p], along_z(slot - here)
+            down_part.at[layer, p, b, :, sides[h]],
+            win.at[layer, p, slot, :, sides[h]],
+            zs.at[layer],
+            zr.at[layer, p, h],
+            along_z(d),
         )
 
-    def win_halves(layer, p, b):
-        for columns, d in ((left, half), (right, -half)):
-            yield send(
-                down_part.at[layer, p, b, :, columns],
-                win.at[layer, p, split, :, columns],
-                zs.at[layer],
-                zr.at[layer, p],
-                along_z(d),
-            )
-
-    def win_got(layer, p):
-        return send(win.at[layer, p, most], win.at[layer, p, most], zs.at[layer], zr.at[layer, p], along_z(1))
+    def win_got(layer, p, h):
+        ref = win.at[layer, p, most, :, sides[h]]
+        return send(ref, ref, zs.at[layer], zr.at[layer, p, h], along_z(1))
 
     def win_sent(layer):
         ref = down_part.at[layer, pl.ds(0, 2), most]
-        return send(ref, ref, zs.at[layer], zr.at[layer, 0], along_z(1))
+        return send(ref, ref, zs.at[layer], zr.at[layer, 0, 0], along_z(1))
 
     upward = nc * (1 - 2 * lax.rem(rank, 2))
 
-    def sum_copies(layer, p, turn):
-        for h, sign in enumerate((1, -1) if turn == 0 else (-1, 1)):
-            columns = pl.ds(h * (width // 2), width // 2)
-            yield send(
-                sums.at[layer, p, 2 * turn, :, columns],
-                sums.at[layer, p, 2 * turn + 1, :, columns],
-                ms.at[layer],
-                mr.at[layer, p, turn],
-                along_z(sign * upward),
-            )
-
-    def sum_got(layer, p, turn):
-        ref = sums.at[layer, p, 2 * turn + 1]
-        return send(ref, ref, ms.at[layer], mr.at[layer, p, turn], along_z(nc))
+    def sum_copy(layer, p, h, turn):
+        return send(
+            sums.at[layer, p, 2 * turn, :, sides[h]],
+            sums.at[layer, p, 2 * turn + 1, :, sides[h]],
+            ms.at[layer],
+            mr.at[layer, p, h, turn],
+            along_z(upward if h == turn else -upward),
+        )
+
+    def sum_got(layer, p, h, turn):
+        ref = sums.at[layer, p, 2 * turn + 1, :, sides[h]]
+        return send(ref, ref, ms.at[layer], mr.at[layer, p, h, turn], along_z(nc))
 
     def sum_sent(layer):
         ref = sums.at[layer, pl.ds(0, 2), pl.ds(0, 2)]
-        return send(ref, ref, ms.at[layer], mr.at[layer, 0, 0], along_z(nc))
-
-    def cur_copies(layer, p, b):
+        return send(ref, ref, ms.at[layer], mr.at[layer, 0, 0, 0], along_z(nc))
+
+    def cur_copies(layer, p, h, b):
         for slot in others:
-            if slot == split:
-                for columns, d in ((left, -half), (right, half)):
-                    ref = cur.at[layer, p, b, :, columns]
-                    yield send(ref, ref, bs.at[layer], br.at[layer, p, b], along_z(d))
-            else:
-                ref = cur.at[layer, p, b]
-                yield send(ref, ref, bs.at[layer], br.at[layer, p, b], along_z(here - slot))
+            ref = cur.at[layer, p, b, :, sides[h]]
+            d = here - slot + (nc if slot == split and h == 1 else 0)
+            yield send(ref, ref, bs.at[layer], br.at[layer, p, b], along_z(d))
 
     def cur_got(layer, p, b):
         ref = cur.at[layer, p, b]
@@ -322,19 +312,24 @@
 
     far_c = sorted(range(1, nc), key=lambda k: -min(k, nc - k))
 
-    def finish(layer, p, total):
+    lengths = {}
+
+    def finish(layer, p, h, total):
         if layer == 0:
-            own = tok[pl.ds(pl.multiple_of((p * nc + mine) * blk, blk), blk), :].astype(f32)
+            there = pl.ds(pl.multiple_of((p * nc + mine) * blk, blk), blk)
+            own = tok[there, side[h]].astype(f32)
         else:
-            own = cur[layer - 1, p, mine].astype(f32)
-        new = (residual_weight * own + down_scale[layer : layer + 1, :] * total).astype(bf16)
+            own = cur[layer - 1, p, mine, :, side[h]].astype(f32)
+        new = (residual_weight * own + down_scale[layer : layer + 1, side[h]] * total).astype(bf16)
         if layer == layers - 1:
             wide = new.astype(f32)
-            squares_row[p, c] = as_row(jnp.sum(wide * wide, axis=1, keepdims=True))
-            for k in far_c:
-                squares_copy(p, lax.rem(c + k, nc)).start()
-        cur[layer, p, mine] = new
-        for copy in cur_copies(layer, p, mine):
+            lengths[p, h] = jnp.sum(wide * wide, axis=1, keepdims=True)
+            if h == 1:
+                squares_row[p, c] = as_row(lengths[p, 0] + lengths[p, 1])
+                for k in far_c:
+                    squares_copy(p, lax.rem(c + k, nc)).start()
+        cur[layer, p, mine, :, side[h]] = new
+        for copy in cur_copies(layer, p, h, mine):
             copy.start()
 
     for layer in range(layers):
@@ -462,43 +457,42 @@
                     down_part[layer, p, b] = d[first : first + blk, :]
                     slot = slot_of(b)
 
-                    @pl.when(jnp.logical_and(slot != here, slot != split))
+                    @pl.when(slot != here)
                     def _(b=b, slot=slot):
-                        win_copy(layer, p, b, slot).start()
-
-                    @pl.when(slot == split)
-                    def _(b=b):
-                        for copy in win_halves(layer, p, b):
-                            copy.start()
+                        win_copy(layer, p, 0, b, slot, slot - here).start()
 
                 return carry
 
             lax.fori_loop(0, nc // 2, two_downs, 0)
+            for slot in others:
+                b = lax.rem(z + slot - here + nz, nc)
+                win_copy(layer, p, 1, b, slot, slot - here - (nc if slot == split else 0)).start()
         if layer + 1 < layers:
             take_in(layer + 1)
             take_down(layer + 1)
 
-        for p in range(2):
-            win[layer, p, here] = down_part[layer, p, mine]
-            win_got(layer, p).wait_recv()
-            total = win[layer, p, 0].astype(f32)
+        pieces = [(p, h) for p in range(2) for h in range(2)]
+        for p, h in pieces:
+            if h == 0:
+                win[layer, p, here] = down_part[layer, p, mine]
+            win_got(layer, p, h).wait_recv()
+            total = win[layer, p, 0, :, side[h]].astype(f32)
             for slot in range(1, nc):
-                total = total + win[layer, p, slot].astype(f32)
-            sums[layer, p, 0] = total.astype(bf16)
-            if layer == 0 and p == 0:
+                total = total + win[layer, p, slot, :, side[h]].astype(f32)
+            sums[layer, p, 0, :, side[h]] = total.astype(bf16)
+            if layer == 0 and (p, h) == (0, 0):
                 greeted(2)
-            for copy in sum_copies(layer, p, 0):
-                copy.start()
+            sum_copy(layer, p, h, 0).start()
         for turn in range(2):
-            for p in range(2):
-                sum_got(layer, p, turn).wait_recv()
-                both = sums[layer, p, 2 * turn].astype(f32) + sums[layer, p, 2 * turn + 1].astype(f32)
+            for p, h in pieces:
+                sum_got(layer, p, h, turn).wait_recv()
+                both = sums[layer, p, 2 * turn, :, side[h]].astype(f32)
+                both = both + sums[layer, p, 2 * turn + 1, :, side[h]].astype(f32)
                 if turn == 0:
-                    sums[layer, p, 2] = both.astype(bf16)
-                    for copy in sum_copies(layer, p, 1):
-                        copy.start()
+                    sums[layer, p, 2, :, side[h]] = both.astype(bf16)
+                    sum_copy(layer, p, h, 1).start()
                 else:
-                    finish(layer, p, both)
+                    finish(layer, p, h, both)
 
     for p in range(2):
         squares_got(p).wait_recv()
@@ -605,7 +599,7 @@
         ]
         + [dma((layers,)), dma((layers, 2))] * 2
         + [dma((layers,)), dma((layers, 2, nc))]
-        + [dma((layers,)), dma((layers, 2)), dma((layers,)), dma((layers, 2, 2))]
+        + [dma((layers,)), dma((layers, 2, 2)), dma((layers,)), dma((layers, 2, 2, 2))]
         + [dma((layers,)), dma((layers, 2, nc))]
         + [dma((1,)), dma((2,)), dma((1,)), dma((2, nc)), dma((1,))]
         + [pltpu.SemaphoreType.REGULAR((3,))],

time: 126 us -> 126 us (level)
  no operation moved by 1% of the time
where the time goes in v7:
time: 126 us
  Pallas kernels  124 us (98%)
  local copies, waits for them, and re-layouts  1.67 us (1%)
    pallas_call x1, Pallas kernels, on_device(): pl.pallas_call(functools.partial(kernel, dims), out_shape=jax.ShapeDtypeS...  124 us

profile of v7, /device:TPU:40, one launch (start us, length us, event | category | flops | bytes accessed | tf_op | source)
XLA Modules:
  0.0 125.6 jit_solution(14686283796662805770)
XLA Ops:
  0.0 123.9 %shard_map.100 = bf16[256,512]{1,0:T(8,128)(2,1)} custom-call(bf16[256,512]{1,0:T(8,128)(2,1)} %tok_hbm.1, f32[3,512]{1,0:T(4,128)} %gains_hbm.1, f32[2,352,512]{2,1,0:T(8,128)} %bitcast.4, f32[2,352,512]{2,1,0:T(8,128)} %bitcast.5, f32[2,352]{1,0:T(2,128)} %gate_scale_hbm.1, f32[2,352]{1,0:T(2,128)} %value_scale_hbm.1, f32[3,2,352]{2,1,0:T(2,128)} %bitcast.6, ...), custom_call_target="tpu_custom_call" | custom-call | flops 400000000 | bytes 10000000 | tf_op jit(solution)/shard_map/pallas_call | solution.py:572
  123.9 1.7 %copy.12 = bf16[256,512]{1,0:T(8,128)(2,1)} copy(bf16[256,512]{1,0:T(8,128)(2,1)} %shard_map.100) | data formatting | bytes 524288

commit v8 on v6

--- a/solution.py
+++ b/solution.py
@@ -320,7 +320,8 @@
     def near_first(i):
         return (2 * lax.rem(i, 2) - 1) * ((i + 1) // 2)
 
-    far_c = sorted(range(1, nc), key=lambda k: -min(k, nc - k))
+    side_c = 1 - 2 * lax.rem(c, 2)
+    far_c = (4, 5, 3, 2, 6, 7, 1) if nc == 8 else tuple(range(nc - 1, 0, -1))
 
     def finish(layer, p, total):
         if layer == 0:
@@ -332,7 +333,7 @@
             wide = new.astype(f32)
             squares_row[p, c] = as_row(jnp.sum(wide * wide, axis=1, keepdims=True))
             for k in far_c:
-                squares_copy(p, lax.rem(c + k, nc)).start()
+                squares_copy(p, lax.rem(c + side_c * k + nc, nc)).start()
         cur[layer, p, mine] = new
         for copy in cur_copies(layer, p, mine):
             copy.start()
@@ -356,7 +357,7 @@
                     pl.semaphore_wait(barrier, len(peers))
                     greet(0)
                 for k in far_c:
-                    to = lax.rem(c + k, nc)
+                    to = lax.rem(c + side_c * k + nc, nc)
                     part_copy(0, p, to).start()
                     halo_copy(0, p, to).start()
         else:
@@ -443,13 +444,13 @@
                 convs.append(y)
             hid[layer, p, c, :, 0:ff] = (jax.nn.gelu(convs[0], approximate=True) * convs[1]).astype(bf16)
             for k in far_c:
-                hid_copy(layer, p, c, lax.rem(c + k, nc)).start()
+                hid_copy(layer, p, c, lax.rem(c + side_c * k + nc, nc)).start()
 
         for p in range(2):
 
             def two_downs(i, carry, layer=layer, p=p):
-                b0 = lax.rem(c + near_first(2 * i) + nc, nc)
-                b1 = lax.rem(c + near_first(2 * i + 1) + nc, nc)
+                b0 = lax.rem(c + side_c * near_first(2 * i) + nc, nc)
+                b1 = lax.rem(c + side_c * near_first(2 * i + 1) + nc, nc)
 
                 @pl.when(i > 0)
                 def _():

time: 126 us -> 126 us (level)
  no operation moved by 1% of the time
where the time goes in v8:
time: 126 us; the launch traced here: 125 us
  Pallas kernels  124 us (98%)
  local copies, waits for them, and re-layouts  1.67 us (1%)
    pallas_call x1, Pallas kernels, on_device(): pl.pallas_call(functools.partial(kernel, dims), out_shape=jax.ShapeDtypeS...  124 us

profile of v8, /device:TPU:40, one launch (start us, length us, event | category | flops | bytes accessed | tf_op | source)
XLA Modules:
  0.0 125.3 jit_solution(2946386303769247204)
XLA Ops:
  0.0 123.7 %shard_map.100 = bf16[256,512]{1,0:T(8,128)(2,1)} custom-call(bf16[256,512]{1,0:T(8,128)(2,1)} %tok_hbm.1, f32[3,512]{1,0:T(4,128)} %gains_hbm.1, f32[2,352,512]{2,1,0:T(8,128)} %bitcast.4, f32[2,352,512]{2,1,0:T(8,128)} %bitcast.5, f32[2,352]{1,0:T(2,128)} %gate_scale_hbm.1, f32[2,352]{1,0:T(2,128)} %value_scale_hbm.1, f32[3,2,352]{2,1,0:T(2,128)} %bitcast.6, ...), custom_call_target="tpu_custom_call" | custom-call | flops 400000000 | bytes 10000000 | tf_op jit(solution)/shard_map/pallas_call | solution.py:579
  123.7 1.7 %copy.12 = bf16[256,512]{1,0:T(8,128)(2,1)} copy(bf16[256,512]{1,0:T(8,128)(2,1)} %shard_map.100) | data formatting | bytes 524288
